TPU v7x, 256 devices: a whole 4x4x8 slice. The times are simulated.
256 devices in a mesh: sp: 64 (over z, x, core), tp: 4 (over y).
Axes of the slice: x: 4, y: 4, z: 8, core: 2. Of those that a mesh axis runs over, the one named last changes fastest.
Arguments:
- out_cotangent: bfloat16 [16384, 2048], P('sp'), may hold values from -16 to 16
- stream: bfloat16 [16384, 2048], P('sp'), may hold values from -6 to 6
- route_ids: int32 [16384, 2], P('sp'), may hold values from 0 to 63, all different within a row; in each aligned block of 256 rows (0 to 255, 256 to 511, ...) at most 16 rows name the same one
- route_weights: float32 [16384, 2], P('sp'), may hold values from 0.3 to 2
- gate_proj: bfloat16 [64, 2048, 1024], P('sp', None, 'tp'), may hold values from -0.125 to 0.125
- up_proj: bfloat16 [64, 2048, 1024], P('sp', None, 'tp'), may hold values from -0.125 to 0.125
- down_proj: bfloat16 [64, 1024, 2048], P('sp', 'tp'), may hold values from -0.1875 to 0.1875
- outer_gate: bfloat16 [16384, 512], P('sp', 'tp'), may hold values from -6 to 6
- inner_gate: bfloat16 [16384, 512], P('sp', 'tp'), may hold values from -6 to 6
- conv_input: bfloat16 [16384, 512], P('sp', 'tp'), may hold values from -6 to 6
- conv_taps: float32 [3, 512], P(None, 'tp'), may hold values from -4 to 4
- out_proj: bfloat16 [2048, 512], P(None, 'tp'), may hold values from -0.25 to 0.25
Outputs:
- grad_gate_proj: bfloat16 [64, 2048, 1024], P('sp', None, 'tp')
- grad_up_proj: bfloat16 [64, 2048, 1024], P('sp', None, 'tp')
- grad_down_proj: bfloat16 [64, 1024, 2048], P('sp', 'tp')
- grad_out_proj: float32 [2048, 512], P('sp', 'tp')
- grad_outer_gate: float32 [16384, 512], P('sp', 'tp')
- grad_inner_gate: float32 [16384, 512], P('sp', 'tp')
- grad_conv_input: float32 [16384, 512], P('sp', 'tp')
Inputs may be any that keep to these rules, and one draw needn't show every extreme that they name: `route_ids`: the 2 experts of a token differ. Among the tokens of one index of sp, no expert is chosen more than 16 times, and in every draw some expert is chosen exactly 16 times by them.
All inputs are finite; a program needn't handle non-finite values.
Results may differ from a plain program's by a relative error of at most 0.018.
Values may be sent and summed in bfloat16 or wider, within the bound.
A program may use at most 64 MiB of HBM per device.

v0:
```python
import jax
import jax.numpy as jnp
from jax import lax
from jax.sharding import PartitionSpec as P


def sent_together(arrays, axis, dim, along):
    widths = [a.shape[along] for a in arrays]
    both = jnp.concatenate(arrays, axis=along)
    out = lax.all_gather(both, axis, axis=dim, tiled=True)
    return tuple(jnp.split(out, [sum(widths[:k]) for k in range(1, len(widths))], axis=along))


def in_blocks(x, dim, devices):
    before, after = (x.shape[:dim], x.shape[dim + 1 :])
    return jnp.moveaxis(x.reshape(*before, devices, -1, *after), dim, 0)


def summed_on_arrival(x, axis, dim):
    pieces = in_blocks(x, dim, lax.axis_size(axis))
    arrived = lax.all_to_all(pieces, axis, split_axis=0, concat_axis=0, tiled=True)
    return arrived.astype(jnp.float32).sum(axis=0)


def sent_to_all(x, axis):
    devices = lax.axis_size(axis)
    return lax.all_to_all(jnp.broadcast_to(x[None], (devices, *x.shape)), axis, 0, 0, tiled=True)


def in_order(pieces, dim):
    shape = list(pieces.shape[1:])
    shape[dim] *= pieces.shape[0]
    return jnp.moveaxis(pieces, 0, dim).reshape(shape)


def gathered_copies(x, axis, dim):
    pieces = sent_to_all(x, axis)
    return in_order(pieces, dim)


def passed_along(x, axis, by):
    devices = lax.axis_size(axis)
    pairs = [(i, i + by) for i in range(devices) if 0 <= i + by < devices]
    return lax.ppermute(x, axis, pairs)


def shards(
    out_cotangent,
    stream,
    route_ids,
    route_weights,
    gate_proj,
    up_proj,
    down_proj,
    outer_gate,
    inner_gate,
    conv_input,
    conv_taps,
    out_proj,
):
    sp_devices = lax.axis_size("sp")
    tokens_here, width = stream.shape
    choices_each = route_ids.shape[1]
    experts = sp_devices * gate_proj.shape[0]
    capacity = 4 * tokens_here // experts
    assigned = tokens_here * choices_each
    flat_expert = route_ids.reshape(-1)
    onehot = (flat_expert[:, None] == jnp.arange(experts, dtype=jnp.int32)[None, :]).astype(
        jnp.int32
    )
    earlier_count = jnp.cumsum(onehot, axis=0) - onehot
    slot_rank = jnp.sum(earlier_count * onehot, axis=1)
    destination = flat_expert * capacity + slot_rank
    slot_source = (
        jnp.full((experts * capacity,), assigned, jnp.int32)
        .at[destination]
        .set(jnp.arange(assigned, dtype=jnp.int32))
    )
    token_of = jnp.arange(assigned, dtype=jnp.int32) // choices_each
    scaled = (
        route_weights.reshape(-1)[:, None] * out_cotangent[token_of].astype(jnp.float32)
    ).astype(jnp.bfloat16)
    zero_row = jnp.zeros((1, width), jnp.bfloat16)
    send_grad = jnp.concatenate([scaled, zero_row], axis=0)[slot_source].reshape(
        sp_devices, capacity, width
    )
    slot_token = jnp.where(slot_source < assigned, slot_source // choices_each, tokens_here)
    send_input = jnp.concatenate([stream, zero_row], axis=0)[slot_token].reshape(
        sp_devices, capacity, width
    )
    columns = width // lax.axis_size("tp")
    offset = lax.axis_index("tp") * columns
    part_grad = lax.dynamic_slice_in_dim(send_grad, offset, columns, 2)
    part_input = lax.dynamic_slice_in_dim(send_input, offset, columns, 2)
    arrived_grad, arrived_input = (
        lax.all_to_all(part_grad, "sp", split_axis=0, concat_axis=0, tiled=True),
        lax.all_to_all(part_input, "sp", split_axis=0, concat_axis=0, tiled=True),
    )
    got_grad, got_input = sent_together((arrived_grad, arrived_input), "tp", 2, 0)
    rows_grad = got_grad.reshape(-1, width)
    rows_input = got_input.reshape(-1, width)
    w_gate = gate_proj[0]
    w_up = up_proj[0]
    w_down = down_proj[0]
    gate = jnp.dot(rows_input, w_gate, preferred_element_type=jnp.float32)
    up = jnp.dot(rows_input, w_up, preferred_element_type=jnp.float32)
    sig = jax.nn.sigmoid(gate)
    silu_gate = gate * sig
    hidden = (silu_gate * up).astype(jnp.bfloat16)
    across = (((1,), (1,)), ((), ()))
    d_hidden = lax.dot_general(rows_grad, w_down, across, preferred_element_type=jnp.float32)
    d_gate = (d_hidden * up * sig * (1.0 + gate * (1.0 - sig))).astype(jnp.bfloat16)
    d_up = (d_hidden * silu_gate).astype(jnp.bfloat16)
    over_rows = (((0,), (0,)), ((), ()))
    grad_down = lax.dot_general(
        hidden, rows_grad, over_rows, preferred_element_type=jnp.float32
    ).astype(jnp.bfloat16)
    grad_gate = lax.dot_general(
        rows_input, d_gate, over_rows, preferred_element_type=jnp.float32
    ).astype(jnp.bfloat16)
    grad_up = lax.dot_general(
        rows_input, d_up, over_rows, preferred_element_type=jnp.float32
    ).astype(jnp.bfloat16)
    partial_input = lax.dot_general(
        d_gate, w_gate, across, preferred_element_type=jnp.float32
    ) + lax.dot_general(d_up, w_up, across, preferred_element_type=jnp.float32)
    share = summed_on_arrival(partial_input.astype(jnp.bfloat16), "tp", 1).astype(jnp.bfloat16)
    quarter = share.shape[1]
    returned = lax.all_to_all(
        share.reshape(sp_devices, capacity, quarter), "sp", split_axis=0, concat_axis=0, tiled=True
    )
    per_assigned = returned.reshape(-1, quarter)[destination].astype(jnp.float32)
    moe_grad = jnp.sum(per_assigned.reshape(tokens_here, choices_each, quarter), axis=1)
    own_cotangent = lax.dynamic_slice_in_dim(
        out_cotangent, lax.axis_index("tp") * quarter, quarter, 1
    )
    stream_part = (own_cotangent.astype(jnp.float32) + moe_grad).astype(jnp.bfloat16)
    stream_grad = gathered_copies(stream_part, "tp", 1)
    mixed = inner_gate.astype(jnp.float32) * conv_input.astype(jnp.float32)
    previous = passed_along(mixed[tokens_here - 2 :], "sp", 1)
    extended = jnp.concatenate([previous, mixed], axis=0)
    conv_out = (
        conv_taps[0] * extended[:tokens_here]
        + conv_taps[1] * extended[1 : tokens_here + 1]
        + conv_taps[2] * extended[2:]
    )
    mixer_out = (outer_gate.astype(jnp.float32) * conv_out).astype(jnp.bfloat16)
    d_mixer = jnp.dot(stream_grad, out_proj, preferred_element_type=jnp.float32)
    grad_outer = d_mixer * conv_out
    d_conv = d_mixer * outer_gate.astype(jnp.float32)
    following = passed_along(d_conv[:2], "sp", -1)
    trailing = jnp.concatenate([d_conv, following], axis=0)
    d_mixed = (
        conv_taps[2] * trailing[:tokens_here]
        + conv_taps[1] * trailing[1 : tokens_here + 1]
        + conv_taps[0] * trailing[2:]
    )
    grad_inner = d_mixed * conv_input.astype(jnp.float32)
    grad_input = d_mixed * inner_gate.astype(jnp.float32)
    columns = stream_grad
    grad_projection = summed_on_arrival(
        lax.dot_general(columns, mixer_out, over_rows, preferred_element_type=jnp.float32).astype(
            jnp.bfloat16
        ),
        "sp",
        0,
    )
    return (
        grad_gate[None],
        grad_up[None],
        grad_down[None],
        grad_projection,
        grad_outer,
        grad_inner,
        grad_input,
    )


def solution(mesh):
    placed = (
        P("sp", None),
        P("sp", None),
        P("sp", None),
        P("sp", None),
        P("sp", None, "tp"),
        P("sp", None, "tp"),
        P("sp", "tp", None),
        P("sp", "tp"),
        P("sp", "tp"),
        P("sp", "tp"),
        P(None, "tp"),
        P(None, "tp"),
    )
    return jax.shard_map(
        shards,
        mesh=mesh,
        in_specs=placed,
        out_specs=(
            P("sp", None, "tp"),
            P("sp", None, "tp"),
            P("sp", "tp", None),
            P("sp", "tp"),
            P("sp", "tp"),
            P("sp", "tp"),
            P("sp", "tp"),
        ),
        check_vma=False,
    )
```

profile of v0, /device:TPU:1, one launch (start us, length us, event | category | flops | bytes accessed | tf_op | source)
XLA Modules:
  0.0 352.2 jit_solution(10132586161418526812)
XLA Ops:
  7.2 0.8 broadcast_multiply_fusion
  8.0 0.8 copy.27
  9.4 1.2 reduce-window.6
  11.0 2.4 scatter_custom_fusion
  13.5 1.3 concatenate.16
  14.8 6.0 %gather_fusion.2 = bf16[1024,2048]{1,0:T(8,128)(2,1)} fusion(bf16[257,2048]{1,0:T(8,128)(2,1)S(1)} %concatenate.16, s32[1024]{0:T(1024)S(1)} %get-tuple-element.17), kind=kCustom, calls=%fused_computation.2 | custom fusion | bytes 8392704 | tf_op jit(solution)/shard_map/gather | solution.py:88
  20.8 2.4 constant_dynamic-slice_fusion
  23.2 13.2 %all-to-all-start.1 = ((bf16[64,16,512]{2,1,0:T(8,128)(2,1)}), bf16[64,16,512]{2,1,0:T(8,128)(2,1)}, u32[]{:S(2)}, u32[]{:S(2)}) async-start(bf16[64,16,512]{2,1,0:T(8,128)(2,1)} %constant_dynamic-slice_fusion), calls=%async_computation.1 | async-start | bytes 2097152 | tf_op jit(solution)/shard_map/all_to_all | solution.py:97
  36.7 3.3 gather_fusion
  40.0 2.0 multiply_convert_fusion
  42.3 6.0 %gather_fusion.1 = bf16[1024,2048]{1,0:T(8,128)(2,1)} fusion(bf16[513,2048]{1,0:T(8,128)(2,1)S(1)} %concatenate.15, s32[1024]{0:T(1024)S(1)} %get-tuple-element.16), kind=kCustom, calls=%fused_computation.1 | custom fusion | bytes 8392704 | tf_op jit(solution)/shard_map/gather | solution.py:84
  48.3 1.3 constant_dynamic-slice_fusion.1
  49.6 14.8 %all-to-all-done.1 = bf16[64,16,512]{2,1,0:T(8,128)(2,1)} async-done(((bf16[64,16,512]{2,1,0:T(8,128)(2,1)}), bf16[64,16,512]{2,1,0:T(8,128)(2,1)}, u32[]{:S(2)}, u32[]{:S(2)}) %all-to-all-start.1) | async-done | bytes 1048608 | tf_op jit(solution)/shard_map/all_to_all | solution.py:97
  64.4 34.2 %all_to_all.30 = bf16[64,16,512]{2,1,0:T(8,128)(2,1)S(1)} all-to-all(bf16[64,16,512]{2,1,0:T(8,128)(2,1)S(1)} %constant_dynamic-slice_fusion.1), channel_id=1, replica_groups=mesh['sp'=64,'tp'=4] {'sp'}, dimensions={0} | all-to-all | bytes 2097152 | tf_op jit(solution)/shard_map/all_to_all | solution.py:96
  98.6 2.8 pad_maximum_fusion
  101.4 82.7 %all-gather.2.cloned.1.call-done = bf16[128,16,2048]{2,1,0:T(8,128)(2,1)} async-done(((bf16[128,16,512]{2,1,0:T(8,128)(2,1)}), bf16[128,16,2048]{2,1,0:T(8,128)(2,1)}) %all-gather.2.cloned.1.call-update) | async-done | bytes 8388624 | tf_op jit(solution)/shard_map/all_gather | solution.py:10
  184.2 4.0 %fusion.41 = (bf16[64,16,2048]{2,1,0:T(8,128)(2,1)S(1)}, bf16[64,16,2048]{2,1,0:T(8,128)(2,1)S(1)}) fusion(bf16[128,16,2048]{2,1,0:T(8,128)(2,1)} %all-gather.2.cloned.1.call-done), kind=kLoop, calls=%fused_computation.93 | loop fusion | bytes 16777216 | tf_op jit(solution)/shard_map/split | solution.py:11
  188.2 1.3 fusion.5
  189.5 0.7 copy-done.5
  190.2 1.3 fusion.8
  191.6 0.6 copy-done.13
  192.2 1.6 multiply_convert_fusion.2
  193.8 1.3 fusion.3
  195.1 1.3 add_convert_fusion
  196.8 51.4 %all_to_all.31 = bf16[4,1024,512]{2,1,0:T(8,128)(2,1)} all-to-all(bf16[4,1024,512]{2,1,0:T(8,128)(2,1)S(1)} %bitcast.81), channel_id=1, replica_groups=mesh['sp'=64,'tp'=4] {'tp'}, dimensions={0} | all-to-all | bytes 8388608 | tf_op jit(solution)/shard_map/all_to_all | solution.py:21
  248.2 4.1 %reduce_sum.43 = bf16[1024,512]{1,0:T(8,128)(2,1)} reduce(bf16[4,1024,512]{2,1,0:T(8,128)(2,1)} %all_to_all.31, bf16[]{:T(256)} %constant.49.clone.1), dimensions={0}, to_apply=%region_4.5 | reduce | flops 1572864 | bytes 5242882 | tf_op jit(solution)/shard_map/reduce_sum | solution.py:22
  252.3 12.0 %all-to-all-start.3 = ((bf16[64,16,512]{2,1,0:T(8,128)(2,1)}), bf16[64,16,512]{2,1,0:T(8,128)(2,1)S(1)}, u32[]{:S(2)}, u32[]{:S(2)}) async-start(bf16[64,16,512]{2,1,0:T(8,128)(2,1)} %bitcast.15), calls=%async_computation.3 | async-start | bytes 2097152 | tf_op jit(solution)/shard_map/all_to_all | solution.py:129
  264.3 28.1 %all-to-all-done.3 = bf16[64,16,512]{2,1,0:T(8,128)(2,1)S(1)} async-done(((bf16[64,16,512]{2,1,0:T(8,128)(2,1)}), bf16[64,16,512]{2,1,0:T(8,128)(2,1)S(1)}, u32[]{:S(2)}, u32[]{:S(2)}) %all-to-all-start.3) | async-done | bytes 1048608 | tf_op jit(solution)/shard_map/all_to_all | solution.py:129
  292.4 2.0 gather_fusion.3
  294.4 0.7 reshape.146
  295.1 1.2 reduce_sum.44
  296.3 1.0 add_convert_fusion.1
  297.5 1.1 broadcast_in_dim.36
  298.6 3.5 all-to-all-start.4
  302.2 4.1 %collective-permute-start = (f32[2,128]{1,0:T(2,128)S(1)}, f32[2,128]{1,0:T(2,128)S(1)}, u32[]{:S(2)}, u32[]{:S(2)}) collective-permute-start(f32[2,128]{1,0:T(2,128)S(1)} %slice.56), channel_id=1, source_target_pairs={{0,4},{4,8},{8,12},{12,16},{16,20},{20,24},{24,28},{28,32},{32,36}... | collective-permute-start | bytes 3080 | tf_op jit(solution)/shard_map/ppermute | solution.py:44
  306.4 5.1 %fusion.2 = bf16[1,256,2048]{2,1,0:T(8,128)(2,1)} fusion(bf16[1024,2048]{1,0:T(8,128)(2,1)} %bitcast.91, f32[1024,256]{1,0:T(8,128)} %copy-done.15, f32[1024,256]{1,0:T(8,128)} %copy-done.14), kind=kOutput, calls=%fused_computation.13 | convolution fusion | flops 1075838976 | bytes 7340032 | tf_op jit(solution)/shard_map/dot_general | solution.py:115
  311.5 4.6 %all-to-all-done.4 = bf16[4,256,512]{1,2,0:T(8,128)(2,1)S(1)} async-done(((bf16[4,256,512]{1,2,0:T(8,128)(2,1)}), bf16[4,256,512]{1,2,0:T(8,128)(2,1)S(1)}, u32[]{:S(2)}, u32[]{:S(2)}) %all-to-all-start.4) | async-done | bytes 1048608 | tf_op jit(solution)/shard_map/all_to_all | solution.py:27
  316.1 2.2 fusion.39
  318.3 1.2 convolution_convert_fusion.3
  319.6 7.4 %all-to-all-start.5 = ((bf16[64,32,128]{2,1,0:T(8,128)(2,1)}), bf16[64,32,128]{2,1,0:T(8,128)(2,1)S(1)}, u32[]{:S(2)}, u32[]{:S(2)}) async-start(bf16[64,32,128]{2,1,0:T(8,128)(2,1)} %bitcast.22), calls=%async_computation.5 | async-start | bytes 1048576 | tf_op jit(solution)/shard_map/all_to_all | solution.py:21
  327.0 4.6 %fusion = bf16[1,2048,256]{2,1,0:T(8,128)(2,1)} fusion(bf16[1024,2048]{1,0:T(8,128)(2,1)} %bitcast.88, bf16[1024,256]{1,0:T(8,128)(2,1)S(1)} %get-tuple-element.14), kind=kOutput, calls=%fused_computation.11 | convolution fusion | flops 1074266112 | bytes 5767168 | tf_op jit(solution)/shard_map/dot_general | solution.py:118
  331.6 2.4 collective-permute-start.1
  334.0 2.4 fusion.1
  336.4 0.4 collective-permute-done.1
  336.8 0.7 convert_multiply_fusion.2
  337.5 0.7 convert_multiply_fusion
  338.2 6.5 %all-to-all-done.5 = bf16[64,32,128]{2,1,0:T(8,128)(2,1)S(1)} async-done(((bf16[64,32,128]{2,1,0:T(8,128)(2,1)}), bf16[64,32,128]{2,1,0:T(8,128)(2,1)S(1)}, u32[]{:S(2)}, u32[]{:S(2)}) %all-to-all-start.5) | async-done | bytes 524320 | tf_op jit(solution)/shard_map/all_to_all | solution.py:21
  344.6 0.7 convert_reduce_fusion
  (57 shorter events, 2.3 us)
Async XLA Ops:
  7.2 181.0 %copy-start = (bf16[1,2048,256]{2,1,0:T(8,128)(2,1)S(1)}, bf16[1,2048,256]{2,1,0:T(8,128)(2,1)}, u32[]{:S(2)}) copy-start(bf16[1,2048,256]{2,1,0:T(8,128)(2,1)} %param.16) | copy-start | bytes 3145732
  20.8 15.6 %copy-start.11 = (f32[256,2]{0,1:T(2,128)S(1)}, f32[256,2]{0,1:T(2,128)}, u32[]{:S(2)}) copy-start(f32[256,2]{0,1:T(2,128)} %param.15) | copy-start | bytes 6148
  20.8 15.9 %copy-start.1 = (bf16[256,2048]{1,0:T(8,128)(2,1)S(1)}, bf16[256,2048]{1,0:T(8,128)(2,1)}, u32[]{:S(2)}) copy-start(bf16[256,2048]{1,0:T(8,128)(2,1)} %param.12) | copy-start | bytes 3145732
  23.2 41.3 %all-to-all-start.1 = ((bf16[64,16,512]{2,1,0:T(8,128)(2,1)}), bf16[64,16,512]{2,1,0:T(8,128)(2,1)}, u32[]{:S(2)}, u32[]{:S(2)}) async-start(bf16[64,16,512]{2,1,0:T(8,128)(2,1)} %constant_dynamic-slice_fusion), calls=%async_computation.1 | async-start | bytes 2097152 | tf_op jit(solution)/shard_map/all_to_all | solution.py:97
  36.3 147.8 %all-gather.2.cloned.1.call-start = ((), (), s32[]{:S(2)}) async-start(), calls=%async_computation.6 | async-start | bytes 10485760 | tf_op jit(solution)/shard_map/all_gather | solution.py:10
  188.2 3.3 copy-start.2
  188.2 3.4 copy-start.4
  188.2 2.0 copy-start.5
  190.2 3.5 %copy-start.14 = (f32[1024,256]{1,0:T(8,128)}, f32[1024,256]{1,0:T(8,128)S(1)}, u32[]{:S(2)}) copy-start(f32[1024,256]{1,0:T(8,128)S(1)} %fusion.5) | copy-start | bytes 3145732
  190.2 2.0 copy-start.13
  191.5 2.3 copy-start.15
  193.8 1.3 copy-start.6
  252.3 40.1 %all-to-all-start.3 = ((bf16[64,16,512]{2,1,0:T(8,128)(2,1)}), bf16[64,16,512]{2,1,0:T(8,128)(2,1)S(1)}, u32[]{:S(2)}, u32[]{:S(2)}) async-start(bf16[64,16,512]{2,1,0:T(8,128)(2,1)} %bitcast.15), calls=%async_computation.3 | async-start | bytes 2097152 | tf_op jit(solution)/shard_map/all_to_all | solution.py:129
  294.4 7.8 %copy-start.9 = (bf16[256,128]{1,0:T(8,128)(2,1)S(1)}, bf16[256,128]{1,0:T(8,128)(2,1)}, u32[]{:S(2)}) copy-start(bf16[256,128]{1,0:T(8,128)(2,1)} %param.21) | copy-start | bytes 196612
  294.4 7.8 %copy-start.10 = (bf16[256,128]{1,0:T(8,128)(2,1)S(1)}, bf16[256,128]{1,0:T(8,128)(2,1)}, u32[]{:S(2)}) copy-start(bf16[256,128]{1,0:T(8,128)(2,1)} %param.20) | copy-start | bytes 196612
  294.4 11.9 %copy-start.12 = (f32[3,128]{1,0:T(4,128)S(1)}, f32[3,128]{1,0:T(4,128)}, u32[]{:S(2)}) copy-start(f32[3,128]{1,0:T(4,128)} %param.22) | copy-start | bytes 4612
  298.6 17.5 %all-to-all-start.4 = ((bf16[4,256,512]{1,2,0:T(8,128)(2,1)}), bf16[4,256,512]{1,2,0:T(8,128)(2,1)S(1)}, u32[]{:S(2)}, u32[]{:S(2)}) async-start(bf16[4,256,512]{1,2,0:T(8,128)(2,1)} %broadcast_in_dim.36), calls=%async_computation.4 | async-start | bytes 2097152 | tf_op jit(solution)/shard_map/all_to_all | solution.py:27
  302.2 9.3 %collective-permute-start = (f32[2,128]{1,0:T(2,128)S(1)}, f32[2,128]{1,0:T(2,128)S(1)}, u32[]{:S(2)}, u32[]{:S(2)}) collective-permute-start(f32[2,128]{1,0:T(2,128)S(1)} %slice.56), channel_id=1, source_target_pairs={{0,4},{4,8},{8,12},{12,16},{16,20},{20,24},{24,28},{28,32},{32,36}... | collective-permute-start | bytes 3080 | tf_op jit(solution)/shard_map/ppermute | solution.py:44
  306.4 9.8 %copy-start.8 = (bf16[256,128]{1,0:T(8,128)(2,1)S(1)}, bf16[256,128]{1,0:T(8,128)(2,1)}, u32[]{:S(2)}) copy-start(bf16[256,128]{1,0:T(8,128)(2,1)} %param.19) | copy-start | bytes 196612
  319.6 25.1 %all-to-all-start.5 = ((bf16[64,32,128]{2,1,0:T(8,128)(2,1)}), bf16[64,32,128]{2,1,0:T(8,128)(2,1)S(1)}, u32[]{:S(2)}, u32[]{:S(2)}) async-start(bf16[64,32,128]{2,1,0:T(8,128)(2,1)} %bitcast.22), calls=%async_computation.5 | async-start | bytes 1048576 | tf_op jit(solution)/shard_map/all_to_all | solution.py:21
  327.0 7.0 %copy-start.3 = (bf16[64,16,2048]{2,1,0:T(8,128)(2,1)S(1)}, bf16[64,16,2048]{2,1,0:T(8,128)(2,1)}, u32[]{:S(2)}) copy-start(bf16[64,16,2048]{2,1,0:T(8,128)(2,1)} %copy-done.2) | copy-start | bytes 12582916
  327.0 7.0 %copy-start.7 = (bf16[1024,256]{1,0:T(8,128)(2,1)S(1)}, bf16[1024,256]{1,0:T(8,128)(2,1)}, u32[]{:S(2)}) copy-start(bf16[1024,256]{1,0:T(8,128)(2,1)} %copy-done.6) | copy-start | bytes 1572868
  331.6 5.2 %collective-permute-start.1 = (f32[2,128]{1,0:T(2,128)S(1)}, f32[2,128]{1,0:T(2,128)S(1)}, u32[]{:S(2)}, u32[]{:S(2)}) collective-permute-start(f32[2,128]{1,0:T(2,128)S(1)} %slice.59), channel_id=1, source_target_pairs={{4,0},{8,4},{12,8},{16,12},{20,16},{24,20},{28,24},{32,28},{36,32}... | collective-permute-start | bytes 3080 | tf_op jit(solution)/shard_map/ppermute | solution.py:44
Sparse Core Ops, SparseCore 0:
  101.6 82.5 all-gather.1
where the time goes:
time: 353 us; the launch traced here: 352 us
  waiting for transfers between devices  137 us (39%)
  blocking collectives  85.6 us (24%)
  starting transfers between devices  42.6 us (12%)
  local copies, waits for them, and re-layouts  34.6 us (10%)
  matrix products  22.2 us (6%)
  other arithmetic  15.4 us (4%)
  between operations  14.5 us (4%)
    all_gather x1, waiting for transfers between devices, sent_together(): out = lax.all_gather(both, axis, axis=dim, tiled=True)  82.7 us
    all_to_all x1, blocking collectives, summed_on_arrival(): lax.all_to_all(pieces, axis, split_axis=0, concat_axis=0, tiled=True)  51.4 us
    all_to_all x1, blocking collectives, shards(): lax.all_to_all(part_grad, 'sp', split_axis=0, concat_axis=0, tiled=True)  34.2 us
    all_to_all x1, waiting for transfers between devices, shards(): lax.all_to_all(share.reshape(sp_devices, capacity, quarter), 'sp', split_...  28.1 us
    all_to_all x1, waiting for transfers between devices, shards(): lax.all_to_all(part_input, 'sp', split_axis=0, concat_axis=0, tiled=True)  14.8 us
    all_to_all x1, starting transfers between devices, shards(): lax.all_to_all(part_input, 'sp', split_axis=0, concat_axis=0, tiled=True)  13.2 us
    all_to_all x1, starting transfers between devices, shards(): lax.all_to_all(share.reshape(sp_devices, capacity, quarter), 'sp', split_...  12 us
    all_to_all x1, starting transfers between devices, summed_on_arrival(): lax.all_to_all(pieces, axis, split_axis=0, concat_axis=0, tiled=True)  7.39 us
  transfers between devices with their start and end apart: 7, of which 6 were waited for; matrix products, arithmetic and copies ran while one was open for 8% of the time, Pallas kernels for 0%

commit v1 on v0

v1 whole, which is shorter than its diff:
```python
import functools

import jax
import jax.numpy as jnp
from jax import lax
from jax.experimental import pallas as pl
from jax.experimental.pallas import tpu as pltpu
from jax.sharding import PartitionSpec as P

MESH = pl.DeviceIdType.MESH
F32 = jnp.float32
BF16 = jnp.bfloat16
NY = 4


def plane_size(sp):
    return 8 if sp % 8 == 0 and sp > 8 else 2


def offsets(n):
    out = []
    for d in range(1, n // 2 + 1):
        out.append(d)
        if n - d != d:
            out.append(n - d)
    return out


def remote(src, dst, send, recv, where):
    return pltpu.make_async_remote_copy(
        src_ref=src, dst_ref=dst, send_sem=send, recv_sem=recv, device_id=where, device_id_type=MESH
    )


class Place:
    def __init__(self, sp_size):
        self.plane = plane_size(sp_size)
        self.depth = sp_size // self.plane
        self.sp = lax.axis_index("sp")
        self.y = lax.axis_index("tp")
        self.z = self.sp // self.plane
        self.a = self.sp % self.plane
        self.up = (self.y + 1) % NY
        self.down = (self.y + NY - 1) % NY
        self.across = (self.y + 2) % NY
        self.dz = offsets(self.depth)
        self.da = list(range(1, self.plane))

    def in_z(self, d):
        return (((self.z + d) % self.depth) * self.plane + self.a, self.y)

    def in_plane(self, d):
        return (self.z * self.plane + (self.a + d) % self.plane, self.y)

    def in_y(self, y):
        return (self.sp, y)

    def meet(self, partners):
        barrier = pltpu.get_barrier_semaphore()
        for where in partners:
            pl.semaphore_signal(barrier, inc=1, device_id=where, device_id_type=MESH)
        pl.semaphore_wait(barrier, len(partners))

    def all_partners(self):
        return (
            [self.in_z(d) for d in self.dz]
            + [self.in_plane(d) for d in self.da]
            + [self.in_y(self.up), self.in_y(self.down)]
        )


def dispatch_kernel(sp_size, snd, rows, zbuf, zs, zr, xs, xr, ys, yr):
    me = Place(sp_size)
    plane, depth = me.plane, me.depth
    cap, quarter = snd.shape[3], snd.shape[4]
    chunk = plane * cap
    me.meet(me.all_partners())

    def columns(y):
        return pl.ds(pl.multiple_of(y * quarter, quarter), quarter)

    sent = []
    along_z = []
    for i, d in enumerate(me.dz):
        copy = remote(snd.at[(me.z + d) % depth], zbuf.at[i], zs.at[i], zr.at[i], me.in_z(d))
        copy.start()
        along_z.append(copy)
        sent.append(copy)

    in_plane = {}

    def spread(i):
        if i == 0:
            block = snd.at[me.z]
        else:
            along_z[i - 1].wait_recv()
            block = zbuf.at[i - 1]
        for j, d in enumerate(me.da):
            target = (me.a + d) % plane
            place = pl.ds((i * plane + d) * cap, cap)
            copy = remote(
                block.at[target],
                rows.at[:, place, columns(me.y)],
                xs.at[i, j],
                xr.at[i, j],
                me.in_plane(d),
            )
            copy.start()
            in_plane[i, j] = copy
            sent.append(copy)
        rows[:, pl.ds(i * chunk, cap), columns(me.y)] = block[me.a]

    direct = {}

    def round_y(i):
        for j in range(len(me.da)):
            in_plane[i, j].wait_recv()
        here = rows.at[:, pl.ds(i * chunk, chunk), columns(me.y)]
        for j, y in enumerate((me.up, me.down)):
            copy = remote(here, here, ys.at[i, j], yr.at[i, j], me.in_y(y))
            copy.start()
            direct[i, j] = copy
            sent.append(copy)

    relayed = {}

    def relay(i):
        for j, (origin, target) in enumerate(((me.down, me.up), (me.up, me.down))):
            direct[i, j].wait_recv()
            piece = rows.at[j, pl.ds(i * chunk, chunk), columns(origin)]
            copy = remote(piece, piece, ys.at[i, 2 + j], yr.at[i, 2 + j], me.in_y(target))
            copy.start()
            relayed[i, j] = copy
            sent.append(copy)

    def finish(i):
        for j in range(2):
            relayed[i, j].wait_recv()

    for step in range(depth + 4):
        if step < depth:
            spread(step)
        if 0 <= step - 1 < depth:
            round_y(step - 1)
        if 0 <= step - 3 < depth:
            relay(step - 3)
        if 0 <= step - 4 < depth:
            finish(step - 4)
    for copy in sent:
        copy.wait_send()


def dispatch(snd, sp_size):
    depth, plane, _, cap, quarter = snd.shape
    rows = depth * plane * cap
    dma = pltpu.SemaphoreType.DMA
    return pl.pallas_call(
        functools.partial(dispatch_kernel, sp_size),
        name="dispatch",
        out_shape=jax.ShapeDtypeStruct((2, rows, NY * quarter), BF16),
        in_specs=[pl.BlockSpec(memory_space=pltpu.VMEM)],
        out_specs=pl.BlockSpec(memory_space=pltpu.VMEM),
        scratch_shapes=[
            pltpu.VMEM((depth - 1, plane, 2, cap, quarter), BF16),
            dma((depth - 1,)),
            dma((depth - 1,)),
            dma((depth, plane - 1)),
            dma((depth, plane - 1)),
            dma((depth, 4)),
            dma((depth, 4)),
        ],
        compiler_params=pltpu.CompilerParams(
            collective_id=0, has_side_effects=True, vmem_limit_bytes=48 * 1024 * 1024
        ),
    )(snd)


def combine_kernel(
    sp_size, part, select, own, out,
    gotup, gotdown, relays, sums, share, retz, ret, moe,
    rs, rr, zs, zr, xs, xr, ys, yr,
):
    me = Place(sp_size)
    plane, depth = me.plane, me.depth
    quarter = own.shape[1]
    cap = part.shape[0] // (depth * plane)
    chunk = plane * cap
    half = chunk // 2
    me.meet(me.all_partners())

    def columns(y):
        return pl.ds(pl.multiple_of(y * quarter, quarter), quarter)

    distances = [0] + me.dz
    order = list(range(depth - 1, -1, -1))
    sent = []
    got = {}

    def first(i):
        low, high = pl.ds(i * chunk, half), pl.ds(i * chunk + half, half)
        lo, hi = pl.ds(0, half), pl.ds(half, half)
        jobs = (
            (0, part.at[low, columns(me.across)], relays.at[i, 0], me.down),
            (1, part.at[high, columns(me.across)], relays.at[i, 1], me.up),
            (2, part.at[high, columns(me.down)], gotup.at[i, hi], me.down),
            (3, part.at[low, columns(me.up)], gotdown.at[i, lo], me.up),
        )
        for j, src, dst, y in jobs:
            copy = remote(src, dst, rs.at[i, j], rr.at[i, j], me.in_y(y))
            copy.start()
            got[i, j] = copy
            sent.append(copy)

    def second(i):
        low, high = pl.ds(i * chunk, half), pl.ds(i * chunk + half, half)
        lo, hi = pl.ds(0, half), pl.ds(half, half)
        got[i, 0].wait_recv()
        sums[i, 0] = (
            part[low, columns(me.down)].astype(F32) + relays[i, 0].astype(F32)
        ).astype(BF16)
        copy = remote(sums.at[i, 0], gotup.at[i, lo], rs.at[i, 4], rr.at[i, 4], me.in_y(me.down))
        copy.start()
        got[i, 4] = copy
        sent.append(copy)
        got[i, 1].wait_recv()
        sums[i, 1] = (
            part[high, columns(me.up)].astype(F32) + relays[i, 1].astype(F32)
        ).astype(BF16)
        copy = remote(sums.at[i, 1], gotdown.at[i, hi], rs.at[i, 5], rr.at[i, 5], me.in_y(me.up))
        copy.start()
        got[i, 5] = copy
        sent.append(copy)

    back = {}

    def third(i):
        for j in range(2, 6):
            got[i, j].wait_recv()
        total = (
            part[pl.ds(i * chunk, chunk), columns(me.y)].astype(F32)
            + gotup[i].astype(F32)
            + gotdown[i].astype(F32)
        ).astype(BF16)
        share[i] = total.reshape(plane, cap, quarter)
        if i > 0:
            d = depth - distances[i]
            copy = remote(share.at[i], retz.at[i - 1], zs.at[i - 1], zr.at[i - 1], me.in_z(d))
            copy.start()
            back[i] = copy
            sent.append(copy)

    spreads = {}

    def fourth(i):
        if i > 0:
            back[i].wait_recv()
            block = retz.at[i - 1]
        else:
            block = share.at[0]
        for d in me.da:
            copy = remote(
                block.at[d], ret.at[i, d], xs.at[i, d - 1], xr.at[i, d - 1],
                me.in_plane(plane - d),
            )
            copy.start()
            spreads[i, d] = copy
            sent.append(copy)
        ret[i, 0] = block[0]

    def fifth(i):
        for d in me.da:
            spreads[i, d].wait_recv()
        place = pl.ds(i * chunk, chunk)
        moe[...] += jnp.dot(
            select[:, place],
            ret[i].reshape(chunk, quarter),
            preferred_element_type=F32,
        )

    moe[...] = own[...].astype(F32)
    first(order[0])
    first(order[1])
    for step in range(depth + 6):
        if step + 2 < depth:
            first(order[step + 2])
        if step < depth:
            second(order[step])
        if 0 <= step - 1 < depth:
            third(order[step - 1])
        if 0 <= step - 3 < depth:
            fourth(order[step - 3])
        if 0 <= step - 4 < depth:
            fifth(order[step - 4])

    parts = ys.shape[0]
    tokens = own.shape[0]
    size = tokens // parts
    out[:, columns(me.y)] = moe[...].astype(BF16)
    direct, relayed = {}, {}
    for k in range(parts):
        here = out.at[pl.ds(k * size, size), columns(me.y)]
        for j, y in enumerate((me.up, me.down)):
            copy = remote(here, here, ys.at[k, j], yr.at[k, j], me.in_y(y))
            copy.start()
            direct[k, j] = copy
            sent.append(copy)
    for k in range(parts):
        for j, (origin, target) in enumerate(((me.down, me.up), (me.up, me.down))):
            direct[k, j].wait_recv()
            piece = out.at[pl.ds(k * size + j * (size // 2), size // 2), columns(origin)]
            copy = remote(piece, piece, ys.at[k, 2 + j], yr.at[k, 2 + j], me.in_y(target))
            copy.start()
            relayed[k, j] = copy
            sent.append(copy)
    for k in range(parts):
        for j in range(2):
            relayed[k, j].wait_recv()
    for copy in sent:
        copy.wait_send()


def combine(part, select, own, sp_size):
    plane = plane_size(sp_size)
    depth = sp_size // plane
    tokens, quarter = own.shape
    slots = part.shape[0]
    cap = slots // sp_size
    chunk = plane * cap
    parts = 4
    dma = pltpu.SemaphoreType.DMA
    return pl.pallas_call(
        functools.partial(combine_kernel, sp_size),
        name="combine",
        out_shape=jax.ShapeDtypeStruct((tokens, NY * quarter), BF16),
        in_specs=[pl.BlockSpec(memory_space=pltpu.VMEM)] * 3,
        out_specs=pl.BlockSpec(memory_space=pltpu.VMEM),
        scratch_shapes=[
            pltpu.VMEM((depth, chunk, quarter), BF16),
            pltpu.VMEM((depth, chunk, quarter), BF16),
            pltpu.VMEM((depth, 2, chunk // 2, quarter), BF16),
            pltpu.VMEM((depth, 2, chunk // 2, quarter), BF16),
            pltpu.VMEM((depth, plane, cap, quarter), BF16),
            pltpu.VMEM((depth - 1, plane, cap, quarter), BF16),
            pltpu.VMEM((depth, plane, cap, quarter), BF16),
            pltpu.VMEM((tokens, quarter), F32),
            dma((depth, 6)),
            dma((depth, 6)),
            dma((depth - 1,)),
            dma((depth - 1,)),
            dma((depth, plane - 1)),
            dma((depth, plane - 1)),
            dma((parts, 4)),
            dma((parts, 4)),
        ],
        compiler_params=pltpu.CompilerParams(
            collective_id=1, has_side_effects=True, vmem_limit_bytes=48 * 1024 * 1024
        ),
    )(part, select, own)


def in_blocks(x, dim, devices):
    before, after = (x.shape[:dim], x.shape[dim + 1 :])
    return jnp.moveaxis(x.reshape(*before, devices, -1, *after), dim, 0)


def summed_on_arrival(x, axis, dim):
    pieces = in_blocks(x, dim, lax.axis_size(axis))
    arrived = lax.all_to_all(pieces, axis, split_axis=0, concat_axis=0, tiled=True)
    return arrived.astype(F32).sum(axis=0)


def passed_along(x, axis, by):
    devices = lax.axis_size(axis)
    pairs = [(i, i + by) for i in range(devices) if 0 <= i + by < devices]
    return lax.ppermute(x, axis, pairs)


def shards(
    out_cotangent,
    stream,
    route_ids,
    route_weights,
    gate_proj,
    up_proj,
    down_proj,
    outer_gate,
    inner_gate,
    conv_input,
    conv_taps,
    out_proj,
):
    sp = lax.axis_size("sp")
    plane = plane_size(sp)
    depth = sp // plane
    tokens, width = stream.shape
    cap = 4 * tokens // sp
    slots = sp * cap
    quarter = width // NY

    ids = route_ids.T
    experts = jnp.arange(sp, dtype=jnp.int32)
    chosen = (ids[:, :, None] == experts).astype(BF16)
    either = chosen[0] + chosen[1]
    row = lax.broadcasted_iota(jnp.int32, (tokens, tokens), 0)
    col = lax.broadcasted_iota(jnp.int32, (tokens, tokens), 1)
    earlier = jnp.dot((col < row).astype(BF16), either, preferred_element_type=F32)
    rank = jnp.sum(chosen.astype(F32) * earlier[None], axis=2).astype(jnp.int32)
    place = ids * cap + rank
    slot = jnp.arange(slots, dtype=jnp.int32)
    hit0 = slot[:, None] == place[0][None, :]
    hit1 = slot[:, None] == place[1][None, :]
    weights = route_weights.T
    slot_weight = jnp.sum(
        jnp.where(hit0, weights[0][None, :], 0.0) + jnp.where(hit1, weights[1][None, :], 0.0), axis=1
    )
    pick = (hit0 | hit1).astype(BF16)
    offset = lax.axis_index("tp") * quarter
    own_cotangent = lax.dynamic_slice_in_dim(out_cotangent, offset, quarter, 1)
    own_stream = lax.dynamic_slice_in_dim(stream, offset, quarter, 1)
    sent_input = jnp.dot(pick, own_stream, preferred_element_type=F32).astype(BF16)
    sent_grad = (
        slot_weight[:, None] * jnp.dot(pick, own_cotangent, preferred_element_type=F32)
    ).astype(BF16)
    snd = jnp.stack(
        [
            sent_input.reshape(depth, plane, cap, quarter),
            sent_grad.reshape(depth, plane, cap, quarter),
        ],
        axis=2,
    )
    got = dispatch(snd, sp)
    rows_input, rows_grad = got[0], got[1]

    w_gate = gate_proj[0]
    w_up = up_proj[0]
    w_down = down_proj[0]
    gate = jnp.dot(rows_input, w_gate, preferred_element_type=F32)
    up = jnp.dot(rows_input, w_up, preferred_element_type=F32)
    sig = jax.nn.sigmoid(gate)
    silu_gate = gate * sig
    hidden = (silu_gate * up).astype(BF16)
    across = (((1,), (1,)), ((), ()))
    d_hidden = lax.dot_general(rows_grad, w_down, across, preferred_element_type=F32)
    d_gate = (d_hidden * up * sig * (1.0 + gate * (1.0 - sig))).astype(BF16)
    d_up = (d_hidden * silu_gate).astype(BF16)
    over_rows = (((0,), (0,)), ((), ()))
    grad_down = lax.dot_general(hidden, rows_grad, over_rows, preferred_element_type=F32).astype(BF16)
    grad_gate = lax.dot_general(rows_input, d_gate, over_rows, preferred_element_type=F32).astype(BF16)
    grad_up = lax.dot_general(rows_input, d_up, over_rows, preferred_element_type=F32).astype(BF16)
    partial_input = (
        lax.dot_general(d_gate, w_gate, across, preferred_element_type=F32)
        + lax.dot_general(d_up, w_up, across, preferred_element_type=F32)
    ).astype(BF16)

    dist = jnp.array([0] + offsets(depth), jnp.int32)
    z = lax.axis_index("sp") // plane
    a = lax.axis_index("sp") % plane
    from_z = (z + dist) % depth
    from_a = (a + jnp.arange(plane, dtype=jnp.int32)) % plane
    expert_of = (from_z[:, None] * plane + from_a[None, :]).reshape(-1)
    slot_at = (expert_of[:, None] * cap + jnp.arange(cap, dtype=jnp.int32)).reshape(-1)
    select = (
        (place[0][:, None] == slot_at[None, :]) | (place[1][:, None] == slot_at[None, :])
    ).astype(BF16)
    stream_grad = combine(partial_input, select, own_cotangent, sp)

    mixed = inner_gate.astype(F32) * conv_input.astype(F32)
    previous = passed_along(mixed[tokens - 2 :], "sp", 1)
    extended = jnp.concatenate([previous, mixed], axis=0)
    conv_out = (
        conv_taps[0] * extended[:tokens]
        + conv_taps[1] * extended[1 : tokens + 1]
        + conv_taps[2] * extended[2:]
    )
    mixer_out = (outer_gate.astype(F32) * conv_out).astype(BF16)
    d_mixer = jnp.dot(stream_grad, out_proj, preferred_element_type=F32)
    grad_outer = d_mixer * conv_out
    d_conv = d_mixer * outer_gate.astype(F32)
    following = passed_along(d_conv[:2], "sp", -1)
    trailing = jnp.concatenate([d_conv, following], axis=0)
    d_mixed = (
        conv_taps[2] * trailing[:tokens]
        + conv_taps[1] * trailing[1 : tokens + 1]
        + conv_taps[0] * trailing[2:]
    )
    grad_inner = d_mixed * conv_input.astype(F32)
    grad_input = d_mixed * inner_gate.astype(F32)
    grad_projection = summed_on_arrival(
        lax.dot_general(stream_grad, mixer_out, over_rows, preferred_element_type=F32).astype(BF16),
        "sp",
        0,
    )
    return (
        grad_gate[None],
        grad_up[None],
        grad_down[None],
        grad_projection,
        grad_outer,
        grad_inner,
        grad_input,
    )


def solution(mesh):
    placed = (
        P("sp", None),
        P("sp", None),
        P("sp", None),
        P("sp", None),
        P("sp", None, "tp"),
        P("sp", None, "tp"),
        P("sp", "tp", None),
        P("sp", "tp"),
        P("sp", "tp"),
        P("sp", "tp"),
        P(None, "tp"),
        P(None, "tp"),
    )
    return jax.shard_map(
        shards,
        mesh=mesh,
        in_specs=placed,
        out_specs=(
            P("sp", None, "tp"),
            P("sp", None, "tp"),
            P("sp", "tp", None),
            P("sp", "tp"),
            P("sp", "tp"),
            P("sp", "tp"),
            P("sp", "tp"),
        ),
        check_vma=False,
    )
```

time: 353 us -> 231 us (0.65)
  Pallas kernels: 0 us -> 164 us
  waiting for transfers between devices: 137 us -> 4.82 us
  blocking collectives: 85.6 us -> 0 us
  local copies, waits for them, and re-layouts: 34.6 us -> 4.53 us
  starting transfers between devices: 42.6 us -> 17.4 us
  between operations: 14.5 us -> 0.88 us
  matrix products: 22.2 us -> 32 us
  other arithmetic: 15.4 us -> 6.67 us
    pallas_call x0 -> x2, Pallas kernels: none -> 164 us  [the longest x1 92.3 us: dispatch(): pl.pallas_call(functools.partial(dispatch_kernel, sp_size), name='dispatc...]
    all_to_all x2 -> x0, blocking collectives: 85.6 us -> none  [the longest x1 51.4 us: summed_on_arrival(): lax.all_to_all(pieces, axis, split_axis=0, concat_axis=0, tiled=True)]
    all_gather x1 -> x0, waiting for transfers between devices: 82.7 us -> none  [sent_together(): out = lax.all_gather(both, axis, axis=dim, tiled=True)]
    all_to_all x3 -> x0, waiting for transfers between devices: 47.6 us -> none  [the longest x1 28.1 us: shards(): lax.all_to_all(share.reshape(sp_devices, capacity, quarter), 'sp', split_...]
    all_to_all x3 -> x0, starting transfers between devices: 28.6 us -> none  [the longest x1 13.2 us: shards(): lax.all_to_all(part_input, 'sp', split_axis=0, concat_axis=0, tiled=True)]
    gather x4 -> x0, local copies, waits for them, and re-layouts: 17.3 us -> none  [the longest x1 6.01 us: shards(): jnp.concatenate([stream, zero_row], axis=0)[slot_token]]
    dot_general x10 -> x13, matrix products: 22.2 us -> 32 us  [the longest x1 4.67 us: shards(): lax.dot_general(d_up, w_up, across, preferred_element_type=F32)]
    reduce_sum x4 -> x3, other arithmetic: 6.18 us -> 1.74 us  [the longest x1 0.75 us: shards(): rank = jnp.sum(chosen.astype(F32) * earlier[None], axis=2).astype(jnp.int32)]
  transfers between devices with their start and end apart: 7 -> 3, of which waited for: 6 -> 1; matrix products, arithmetic and copies ran while one was open for 8% -> 16% of each run, Pallas kernels for 0% -> 71%
where the time goes in v1:
time: 231 us; the launch traced here: 230 us
  Pallas kernels  164 us (71%)
  matrix products  32 us (14%)
  starting transfers between devices  17.4 us (8%)
  other arithmetic  6.67 us (3%)
  waiting for transfers between devices  4.82 us (2%)
  local copies, waits for them, and re-layouts  4.53 us (2%)
    pallas_call x1, Pallas kernels, dispatch(): pl.pallas_call(functools.partial(dispatch_kernel, sp_size), name='dispatc...  92.3 us
    pallas_call x1, Pallas kernels, combine(): pl.pallas_call(functools.partial(combine_kernel, sp_size), name='combine'...  71.7 us
    all_to_all x1, starting transfers between devices, summed_on_arrival(): lax.all_to_all(pieces, axis, split_axis=0, concat_axis=0, tiled=True)  10.4 us
    ppermute x2, starting transfers between devices, passed_along(): return lax.ppermute(x, axis, pairs)  6.98 us
    all_to_all x1, waiting for transfers between devices, summed_on_arrival(): lax.all_to_all(pieces, axis, split_axis=0, concat_axis=0, tiled=True)  4.81 us
    dot_general x1, matrix products, shards(): lax.dot_general(d_up, w_up, across, preferred_element_type=F32)  4.67 us
  transfers between devices with their start and end apart: 3, of which 1 were waited for; matrix products, arithmetic and copies ran while one was open for 16% of the time, Pallas kernels for 71%

profile of v1, /device:TPU:1, one launch (start us, length us, event | category | flops | bytes accessed | tf_op | source)
XLA Modules:
  0.0 230.4 jit_solution(4383704591474350422)
XLA Ops:
  0.6 0.0 copy-start
  0.6 1.0 convert_multiply_fusion.1
  1.6 0.6 slice.79
  2.2 4.5 %collective-permute-start = (f32[2,128]{1,0:T(2,128)}, f32[2,128]{1,0:T(2,128)}, u32[]{:S(2)}, u32[]{:S(2)}) collective-permute-start(f32[2,128]{1,0:T(2,128)} %slice.79), channel_id=1, source_target_pairs={{0,4},{4,8},{8,12},{12,16},{16,20},{20,24},{24,28},{28,32},{32,36}... | collective-permute-start | bytes 3080 | tf_op jit(solution)/shard_map/ppermute | solution.py:375
  6.7 0.8 fusion.78
  7.5 0.7 fusion.64
  8.2 0.2 fusion.51
  8.3 0.7 multiply_reduce_fusion
  9.1 0.7 convert_add_fusion
  9.8 1.0 constant_dynamic-slice_fusion.own
  10.7 1.4 convolution_convert_fusion.1
  12.1 0.3 add_reduce_fusion
  12.4 0.5 multiply_convert_fusion
  12.9 0.2 pad_maximum_fusion.snd
  13.1 92.3 %dispatch.1 = bf16[2,1024,2048]{2,1,0:T(8,128)(2,1)} custom-call(bf16[8,8,2,16,512]{4,3,2,1,0:T(8,128)(2,1)S(1)} %pad_maximum_fusion.snd), custom_call_target="tpu_custom_call" | custom-call | tf_op jit(solution)/shard_map/dispatch/pallas_call | solution.py:157
  105.4 0.0 copy-done
  105.4 0.0 copy-start.2
  105.5 3.6 %fusion.8 = f32[1024,256]{1,0:T(8,128)S(1)} fusion(bf16[2,1024,2048]{2,1,0:T(8,128)(2,1)} %dispatch.1, bf16[1,2048,256]{2,1,0:T(8,128)(2,1)S(1)} %copy-done), kind=kOutput, calls=%fused_computation.9 | convolution fusion | flops 1073741824 | bytes 6291456 | tf_op jit(solution)/shard_map/dot_general | solution.py:437
  109.1 1.0 copy-done.1
  110.1 0.2 copy-done.2
  110.3 1.3 fusion.10
  111.6 0.0 copy-start.9
  111.6 2.3 %fusion.27 = bf16[1,256,2048]{2,1,0:T(8,128)(2,1)} fusion(bf16[2,1024,2048]{2,1,0:T(8,128)(2,1)S(1)} %copy-done.1, f32[1024,256]{1,0:T(8,128)S(1)} %fusion.10, f32[1024,256]{1,0:T(8,128)S(1)} %fusion.8), kind=kOutput, calls=%fused_computation.22 | convolution fusion | flops 1075838976 | bytes 7340032 | tf_op jit(solution)/shard_map/dot_general | solution.py:447
  113.9 1.6 multiply_convert_fusion.2
  115.5 0.0 copy-start.8
  115.5 4.5 %fusion.36 = f32[1024,2048]{1,0:T(8,128)} fusion(bf16[1024,256]{1,0:T(8,128)(2,1)S(1)} %get-tuple-element.12, bf16[1,2048,256]{2,1,0:T(8,128)(2,1)S(1)} %copy-done), kind=kOutput, calls=%fused_computation.29 | convolution fusion | flops 1073741824 | bytes 9961472 | tf_op jit(solution)/shard_map/dot_general | solution.py:451
  120.0 0.1 add_multiply_fusion
  120.1 0.1 mul.147
  120.2 0.7 iota_add_fusion
  120.9 0.8 add.132
  121.7 0.2 or_convert_fusion.select
  121.9 0.0 copy-start.7
  121.9 4.7 %add_convert_fusion.part = bf16[1024,2048]{1,0:T(8,128)(2,1)S(1)} fusion(f32[1024,2048]{1,0:T(8,128)} %fusion.36, bf16[1024,256]{1,0:T(8,128)(2,1)S(1)} %get-tuple-element.11, bf16[1,2048,256]{2,1,0:T(8,128)(2,1)S(1)} %copy-done.2), kind=kOutput, calls=%fused_computation | convolution fusion | flops 1077936128 | bytes 14155776 | tf_op jit(solution)/shard_map/dot_general | solution.py:452
  126.6 0.0 copy-start.3
  126.6 0.0 copy-start.4
  126.7 71.7 %combine.1 = bf16[256,2048]{1,0:T(8,128)(2,1)S(1)} custom-call(bf16[1024,2048]{1,0:T(8,128)(2,1)S(1)} %add_convert_fusion.part, bf16[256,1024]{1,0:T(8,128)(2,1)S(1)} %or_convert_fusion.select, bf16[256,512]{1,0:T(8,128)(2,1)S(1)} %constant_dynamic-slice_fusion.own), custom_call_target="tpu_custom_call" | custom-call | tf_op jit(solution)/shard_map/combine/pallas_call | solution.py:331
  198.4 0.0 collective-permute-done
  198.4 1.8 fusion.75
  200.2 1.3 convolution_convert_fusion
  201.5 10.4 %all-to-all-start = ((bf16[64,32,128]{2,1,0:T(8,128)(2,1)}), bf16[64,32,128]{2,1,0:T(8,128)(2,1)S(1)}, u32[]{:S(2)}, u32[]{:S(2)}) async-start(bf16[64,32,128]{2,1,0:T(8,128)(2,1)} %bitcast.20), calls=%async_computation | async-start | bytes 1048576 | tf_op jit(solution)/shard_map/all_to_all | solution.py:368
  212.0 4.5 %fusion.33 = bf16[1,2048,256]{2,1,0:T(8,128)(2,1)} fusion(bf16[1024,256]{1,0:T(8,128)(2,1)S(1)} %get-tuple-element.12, bf16[2,1024,2048]{2,1,0:T(8,128)(2,1)} %dispatch.1), kind=kOutput, calls=%fused_computation.24 | convolution fusion | flops 1074266112 | bytes 5767168 | tf_op jit(solution)/shard_map/dot_general | solution.py:448
  216.5 2.5 %collective-permute-start.1 = (f32[2,128]{1,0:T(2,128)S(1)}, f32[2,128]{1,0:T(2,128)S(1)}, u32[]{:S(2)}, u32[]{:S(2)}) collective-permute-start(f32[2,128]{1,0:T(2,128)S(1)} %slice.82), channel_id=1, source_target_pairs={{4,0},{8,4},{12,8},{16,12},{20,16},{24,20},{28,24},{32,28},{36,32}... | collective-permute-start | bytes 3080 | tf_op jit(solution)/shard_map/ppermute | solution.py:375
  219.0 4.5 %fusion.30 = bf16[1,2048,256]{2,1,0:T(8,128)(2,1)} fusion(bf16[1024,256]{1,0:T(8,128)(2,1)S(1)} %get-tuple-element.11, bf16[2,1024,2048]{2,1,0:T(8,128)(2,1)} %dispatch.1), kind=kOutput, calls=%fused_computation.23 | convolution fusion | flops 1074266112 | bytes 5767168 | tf_op jit(solution)/shard_map/dot_general | solution.py:449
  223.5 0.0 collective-permute-done.1
  223.5 0.7 convert_multiply_fusion.2
  224.2 0.7 convert_multiply_fusion
  224.8 4.8 %all-to-all-done = bf16[64,32,128]{2,1,0:T(8,128)(2,1)S(1)} async-done(((bf16[64,32,128]{2,1,0:T(8,128)(2,1)}), bf16[64,32,128]{2,1,0:T(8,128)(2,1)S(1)}, u32[]{:S(2)}, u32[]{:S(2)}) %all-to-all-start) | async-done | bytes 524320 | tf_op jit(solution)/shard_map/all_to_all | solution.py:368
  229.7 0.7 convert_reduce_fusion
  (14 shorter events, 0.0 us)
Async XLA Ops:
  0.6 104.8 %copy-start = (bf16[1,2048,256]{2,1,0:T(8,128)(2,1)S(1)}, bf16[1,2048,256]{2,1,0:T(8,128)(2,1)}, u32[]{:S(2)}) copy-start(bf16[1,2048,256]{2,1,0:T(8,128)(2,1)} %param.17) | copy-start | bytes 3145732
  2.2 196.2 %collective-permute-start = (f32[2,128]{1,0:T(2,128)}, f32[2,128]{1,0:T(2,128)}, u32[]{:S(2)}, u32[]{:S(2)}) collective-permute-start(f32[2,128]{1,0:T(2,128)} %slice.79), channel_id=1, source_target_pairs={{0,4},{4,8},{8,12},{12,16},{16,20},{20,24},{24,28},{28,32},{32,36}... | collective-permute-start | bytes 3080 | tf_op jit(solution)/shard_map/ppermute | solution.py:375
  105.4 4.6 %copy-start.1 = (bf16[2,1024,2048]{2,1,0:T(8,128)(2,1)S(1)}, bf16[2,1024,2048]{2,1,0:T(8,128)(2,1)}, u32[]{:S(2)}) copy-start(bf16[2,1024,2048]{2,1,0:T(8,128)(2,1)} %dispatch.1) | copy-start | bytes 25165828
  105.4 4.9 %copy-start.2 = (bf16[1,2048,256]{2,1,0:T(8,128)(2,1)S(1)}, bf16[1,2048,256]{2,1,0:T(8,128)(2,1)}, u32[]{:S(2)}) copy-start(bf16[1,2048,256]{2,1,0:T(8,128)(2,1)} %param.18) | copy-start | bytes 3145732
  111.6 2.3 %copy-start.9 = (bf16[1,256,2048]{2,1,0:T(8,128)(2,1)S(1)}, bf16[1,256,2048]{2,1,0:T(8,128)(2,1)}, u32[]{:S(2)}) copy-start(bf16[1,256,2048]{2,1,0:T(8,128)(2,1)} %param.19) | copy-start | bytes 3145732
  115.5 4.5 %copy-start.8 = (s32[8]{0:T(128)S(1)}, s32[8]{0:T(128)}, u32[]{:S(2)}) copy-start(s32[8]{0:T(128)} %constant.63.clone) | copy-start | bytes 100
  121.9 4.7 %copy-start.7 = (f32[3,128]{1,0:T(4,128)S(1)}, f32[3,128]{1,0:T(4,128)}, u32[]{:S(2)}) copy-start(f32[3,128]{1,0:T(4,128)} %param.23) | copy-start | bytes 4612
  126.6 71.7 %copy-start.3 = (bf16[2048,128]{1,0:T(8,128)(2,1)S(1)}, bf16[2048,128]{1,0:T(8,128)(2,1)}, u32[]{:S(2)}) copy-start(bf16[2048,128]{1,0:T(8,128)(2,1)} %param.24) | copy-start | bytes 1572868
  126.6 71.7 %copy-start.4 = (bf16[256,128]{1,0:T(8,128)(2,1)S(1)}, bf16[256,128]{1,0:T(8,128)(2,1)}, u32[]{:S(2)}) copy-start(bf16[256,128]{1,0:T(8,128)(2,1)} %param.20) | copy-start | bytes 196612
  201.5 28.1 %all-to-all-start = ((bf16[64,32,128]{2,1,0:T(8,128)(2,1)}), bf16[64,32,128]{2,1,0:T(8,128)(2,1)S(1)}, u32[]{:S(2)}, u32[]{:S(2)}) async-start(bf16[64,32,128]{2,1,0:T(8,128)(2,1)} %bitcast.20), calls=%async_computation | async-start | bytes 1048576 | tf_op jit(solution)/shard_map/all_to_all | solution.py:368
  216.5 7.0 %copy-start.6 = (bf16[256,128]{1,0:T(8,128)(2,1)S(1)}, bf16[256,128]{1,0:T(8,128)(2,1)}, u32[]{:S(2)}) copy-start(bf16[256,128]{1,0:T(8,128)(2,1)} %param.21) | copy-start | bytes 196612
  216.5 7.7 %copy-start.5 = (bf16[256,128]{1,0:T(8,128)(2,1)S(1)}, bf16[256,128]{1,0:T(8,128)(2,1)}, u32[]{:S(2)}) copy-start(bf16[256,128]{1,0:T(8,128)(2,1)} %param.22) | copy-start | bytes 196612
  216.5 7.0 %collective-permute-start.1 = (f32[2,128]{1,0:T(2,128)S(1)}, f32[2,128]{1,0:T(2,128)S(1)}, u32[]{:S(2)}, u32[]{:S(2)}) collective-permute-start(f32[2,128]{1,0:T(2,128)S(1)} %slice.82), channel_id=1, source_target_pairs={{4,0},{8,4},{12,8},{16,12},{20,16},{24,20},{28,24},{32,28},{36,32}... | collective-permute-start | bytes 3080 | tf_op jit(solution)/shard_map/ppermute | solution.py:375

commit v2 on v0

v2 whole, which is shorter than its diff:
```python
import functools

import jax
import jax.numpy as jnp
from jax import lax
from jax.experimental import pallas as pl
from jax.experimental.pallas import tpu as pltpu
from jax.sharding import PartitionSpec as P

MESH = pl.DeviceIdType.MESH
F32 = jnp.float32
BF16 = jnp.bfloat16
NY = 4


def plane_size(sp):
    return 8 if sp % 8 == 0 and sp > 8 else 2


def offsets(n):
    out = []
    for d in range(1, n // 2 + 1):
        out.append(d)
        if n - d != d:
            out.append(n - d)
    return out


def remote(src, dst, send, recv, where):
    return pltpu.make_async_remote_copy(
        src_ref=src, dst_ref=dst, send_sem=send, recv_sem=recv, device_id=where, device_id_type=MESH
    )


class Place:
    def __init__(self, sp_size):
        self.plane = plane_size(sp_size)
        self.depth = sp_size // self.plane
        self.sp = lax.axis_index("sp")
        self.y = lax.axis_index("tp")
        self.z = self.sp // self.plane
        self.a = self.sp % self.plane
        self.up = (self.y + 1) % NY
        self.down = (self.y + NY - 1) % NY
        self.across = (self.y + 2) % NY
        self.dz = offsets(self.depth)
        self.da = list(range(1, self.plane))

    def in_z(self, d):
        return (((self.z + d) % self.depth) * self.plane + self.a, self.y)

    def in_plane(self, d):
        return (self.z * self.plane + (self.a + d) % self.plane, self.y)

    def in_y(self, y):
        return (self.sp, y)

    def meet(self, partners):
        barrier = pltpu.get_barrier_semaphore()
        for where in partners:
            pl.semaphore_signal(barrier, inc=1, device_id=where, device_id_type=MESH)
        pl.semaphore_wait(barrier, len(partners))

    def all_partners(self):
        return (
            [self.in_z(d) for d in self.dz]
            + [self.in_plane(d) for d in self.da]
            + [self.in_y(self.up), self.in_y(self.down)]
        )


ORDERS = {
    8: "B0 S0 B1 B2 B3 B4 Y0 B5 B6 B7 S1 S2 R0 Y1 Y2 R1 S3 S4 Y3 Y4 R2 F0 F1 D0 S5 S6 R3 Y5 Y6 R4 "
    "F2 F3 D1 S7 Y7 R5 R6 F4 F5 D2 R7 F6 F7 D3",
    2: "B0 S0 B1 Y0 S1 R0 Y1 R1 F0 F1 D0",
}
NT = (((1,), (1,)), ((), ()))
TN = (((0,), (0,)), ((), ()))


def layer_kernel(
    sp_size,
    cap,
    ids, weights, outer, inner, convin, taps,
    cotangent, stream, w_gate, w_up, w_down, w_out,
    g_gate, g_up, g_down, g_out, g_outer, g_inner, g_convin,
    xq, ctq, scaled, wgu, wd, wo,
    snd, zbuf, rows, hid, dgu, part,
    gotup, gotdown, relays, sums, share, retz, ret, moe, out,
    ext, dext, mixer, conv, gp, cbuf, hx, xbuf, hz, zsum,
    local, zs, zr, xs, xr, ys, yr, rs, rr, bs, br, ps, pr, as_, ar, hs, hr, cs, cr, gs, gr, ts, tr,
):
    me = Place(sp_size)
    plane, depth = me.plane, me.depth
    tokens, quarter = xq.shape
    width = quarter * NY
    hidden = wd.shape[0]
    chunk = plane * cap
    half = chunk // 2
    slots = depth * chunk
    distances = [0] + me.dz
    after, before = ((me.sp + 1) % sp_size, me.y), ((me.sp + sp_size - 1) % sp_size, me.y)
    sent = []

    def columns(y):
        return pl.ds(pl.multiple_of(y * quarter, quarter), quarter)

    def send(src, dst, send_sem, recv_sem, where):
        copy = remote(src, dst, send_sem, recv_sem, where)
        copy.start()
        sent.append(copy)
        return copy

    loads = [
        pltpu.make_async_copy(stream.at[:, columns(me.y)], xq, local.at[0]),
        pltpu.make_async_copy(cotangent.at[:, columns(me.y)], ctq, local.at[1]),
        pltpu.make_async_copy(w_gate, wgu.at[:, pl.ds(0, hidden)], local.at[2]),
        pltpu.make_async_copy(w_up, wgu.at[:, pl.ds(hidden, hidden)], local.at[3]),
        pltpu.make_async_copy(w_down, wd, local.at[4]),
        pltpu.make_async_copy(w_out, wo, local.at[5]),
    ]
    for copy in loads:
        copy.start()

    barrier = pltpu.get_barrier_semaphore()
    partners = me.all_partners() + [after, before]
    for where in partners:
        pl.semaphore_signal(barrier, inc=1, device_id=where, device_id_type=MESH)

    def iota(shape, dim):
        return lax.broadcasted_iota(jnp.int32, shape, dim)

    square = (tokens, tokens)
    row, col = iota(square, 0), iota(square, 1)
    ids_col = ids[...]
    ids_row = lax.dot_general(
        ids_col.astype(F32).astype(BF16), (row == col).astype(F32).astype(BF16), TN, preferred_element_type=F32
    ).astype(jnp.int32)
    by_col = [
        (iota((tokens, sp_size), 1) == ids_col[:, k : k + 1]).astype(F32) for k in range(2)
    ]
    by_row = [
        (iota((sp_size, tokens), 0) == ids_row[k : k + 1, :]).astype(F32) for k in range(2)
    ]
    count_col = jnp.dot(
        (col < row).astype(F32).astype(BF16), (by_col[0] + by_col[1]).astype(BF16),
        preferred_element_type=F32,
    )
    count_row = jnp.dot(
        (by_row[0] + by_row[1]).astype(BF16), (row < col).astype(F32).astype(BF16),
        preferred_element_type=F32,
    )
    place_col, place_row = [], []
    for k in range(2):
        rank = jnp.sum(by_col[k] * count_col, axis=1, keepdims=True).astype(jnp.int32)
        place_col.append(ids_col[:, k : k + 1] * cap + rank)
        rank = jnp.sum(by_row[k] * count_row, axis=0, keepdims=True).astype(jnp.int32)
        place_row.append(ids_row[k : k + 1, :] * cap + rank)

    mixed = inner[...].astype(F32) * convin[...].astype(F32)
    ext[pl.ds(8, tokens), :] = mixed

    loads[0].wait()
    loads[1].wait()
    for k in range(2):
        scaled[pl.ds(k * tokens, tokens), :] = (
            weights[:, k : k + 1] * ctq[...].astype(F32)
        ).astype(BF16)

    pl.semaphore_wait(barrier, len(partners))

    def base(i):
        return ((me.z + distances[i]) % depth) * chunk

    along_z = {}

    def build(i):
        slot = base(i) + iota((chunk, tokens), 0)
        hits = [(slot == place_row[k]).astype(F32) for k in range(2)]
        picked = jnp.dot(
            (hits[0] + hits[1]).astype(BF16), xq[...], preferred_element_type=F32
        ).astype(BF16)
        snd[i, :, 0] = picked.reshape(plane, cap, quarter)
        picked = jnp.dot(
            jnp.concatenate(hits, axis=1).astype(BF16), scaled[...], preferred_element_type=F32
        ).astype(BF16)
        snd[i, :, 1] = picked.reshape(plane, cap, quarter)
        if i > 0:
            along_z[i] = send(
                snd.at[i], zbuf.at[i - 1], zs.at[i - 1], zr.at[i - 1], me.in_z(distances[i])
            )

    in_plane = {}

    def spread(i):
        if i == 0:
            block = snd.at[0]
        else:
            along_z[i].wait_recv()
            block = zbuf.at[i - 1]
        for d in me.da:
            in_plane[i, d] = send(
                block.at[(me.a + d) % plane],
                rows.at[:, pl.ds((i * plane + d) * cap, cap), columns(me.y)],
                xs.at[i, d - 1],
                xr.at[i, d - 1],
                me.in_plane(d),
            )
        rows[:, pl.ds(i * chunk, cap), columns(me.y)] = block[me.a]

    direct, relayed = {}, {}

    def round_y(i):
        for d in me.da:
            in_plane[i, d].wait_recv()
        here = rows.at[:, pl.ds(i * chunk, chunk), columns(me.y)]
        for j, y in enumerate((me.up, me.down)):
            direct[i, j] = send(here, here, ys.at[i, j], yr.at[i, j], me.in_y(y))

    def relay(i):
        for j, (origin, target) in enumerate(((me.down, me.up), (me.up, me.down))):
            direct[i, j].wait_recv()
            piece = rows.at[j, pl.ds(i * chunk, chunk), columns(origin)]
            relayed[i, j] = send(piece, piece, ys.at[i, 2 + j], yr.at[i, 2 + j], me.in_y(target))

    def finish(i):
        for j in range(2):
            relayed[i, j].wait_recv()

    def expert(g):
        if g == 0:
            for k in range(2, 5):
                loads[k].wait()
        here = pl.ds(g * 2 * chunk, 2 * chunk)
        both = jnp.dot(rows[0, here, :], wgu[...], preferred_element_type=F32)
        gate, up = both[:, :hidden], both[:, hidden:]
        d_hidden = lax.dot_general(rows[1, here, :], wd[...], NT, preferred_element_type=F32)
        sig = jax.nn.sigmoid(gate)
        silu = gate * sig
        hid[here, :] = (silu * up).astype(BF16)
        dgu[here, pl.ds(0, hidden)] = (d_hidden * up * sig * (1.0 + gate * (1.0 - sig))).astype(BF16)
        dgu[here, pl.ds(hidden, hidden)] = (d_hidden * silu).astype(BF16)
        part[here, :] = lax.dot_general(
            dgu[here, :], wgu[...], NT, preferred_element_type=F32
        ).astype(BF16)

    jobs = {"B": build, "S": spread, "Y": round_y, "R": relay, "F": finish, "D": expert}
    for name in ORDERS[depth].split():
        jobs[name[0]](int(name[1:]))

    got = {}

    def first(i):
        low, high = pl.ds(i * chunk, half), pl.ds(i * chunk + half, half)
        lo, hi = pl.ds(0, half), pl.ds(half, half)
        for j, src, dst, y in (
            (0, part.at[low, columns(me.across)], relays.at[i, 0], me.down),
            (1, part.at[high, columns(me.across)], relays.at[i, 1], me.up),
            (2, part.at[high, columns(me.down)], gotup.at[i, hi], me.down),
            (3, part.at[low, columns(me.up)], gotdown.at[i, lo], me.up),
        ):
            got[i, j] = send(src, dst, rs.at[i, j], rr.at[i, j], me.in_y(y))

    def second(i):
        low, high = pl.ds(i * chunk, half), pl.ds(i * chunk + half, half)
        lo, hi = pl.ds(0, half), pl.ds(half, half)
        for j, mine, y, dst in (
            (0, low, me.down, gotup.at[i, lo]),
            (1, high, me.up, gotdown.at[i, hi]),
        ):
            got[i, j].wait_recv()
            sums[i, j] = (
                part[mine, columns(y)].astype(F32) + relays[i, j].astype(F32)
            ).astype(BF16)
            got[i, 4 + j] = send(sums.at[i, j], dst, rs.at[i, 4 + j], rr.at[i, 4 + j], me.in_y(y))

    back = {}

    def third(i):
        for j in range(2, 6):
            got[i, j].wait_recv()
        total = (
            part[pl.ds(i * chunk, chunk), columns(me.y)].astype(F32)
            + gotup[i].astype(F32)
            + gotdown[i].astype(F32)
        ).astype(BF16)
        share[i] = total.reshape(plane, cap, quarter)
        if i > 0:
            back[i] = send(
                share.at[i], retz.at[i - 1], bs.at[i - 1], br.at[i - 1],
                me.in_z(depth - distances[i]),
            )

    spreads = {}

    def fourth(i):
        if i > 0:
            back[i].wait_recv()
            block = retz.at[i - 1]
        else:
            block = share.at[0]
        for d in me.da:
            spreads[i, d] = send(
                block.at[d], ret.at[i, me.a], ps.at[i, d - 1], pr.at[i, d - 1],
                me.in_plane(plane - d),
            )
        ret[i, me.a] = block[0]

    def fifth(i):
        for d in me.da:
            spreads[i, d].wait_recv()
        slot = base(i) + iota((tokens, chunk), 1)
        hit = ((slot == place_col[0]) | (slot == place_col[1])).astype(F32).astype(BF16)
        moe[...] += jnp.dot(hit, ret[i].reshape(chunk, quarter), preferred_element_type=F32)

    tiles = depth
    wide = width // tiles

    def weight_grads(t):
        cols = pl.ds(t * wide, wide)
        both = lax.dot_general(rows[0, :, cols], dgu[...], TN, preferred_element_type=F32)
        g_gate[cols, :] = both[:, :hidden].astype(BF16)
        g_up[cols, :] = both[:, hidden:].astype(BF16)
        g_down[:, cols] = lax.dot_general(
            hid[...], rows[1, :, cols], TN, preferred_element_type=F32
        ).astype(BF16)

    def convolution():
        halo.wait_recv()
        ext[pl.ds(0, 8), :] = jnp.where(me.sp == 0, 0.0, ext[pl.ds(0, 8), :])
        conv_out = (
            taps[0:1, :] * ext[pl.ds(6, tokens), :]
            + taps[1:2, :] * ext[pl.ds(7, tokens), :]
            + taps[2:3, :] * ext[pl.ds(8, tokens), :]
        )
        conv[...] = conv_out
        mixer[...] = (outer[...].astype(F32) * conv_out).astype(BF16)

    order = list(range(depth - 1, -1, -1))
    moe[...] = ctq[...].astype(F32)
    first(order[0])
    first(order[1])
    halo = send(ext.at[pl.ds(tokens, 8)], ext.at[pl.ds(0, 8)], hs.at[0], hr.at[0], after)
    for step in range(depth + 1):
        if step + 2 < depth:
            first(order[step + 2])
        if step < depth:
            second(order[step])
        if step >= 1:
            third(order[step - 1])
        if step < tiles:
            weight_grads(step)
        if step == 1:
            convolution()
        if step >= 5:
            fourth(order[step - 5])
        if step >= 6:
            fifth(order[step - 6])
    begun = max(depth + 1 - 5, 0)
    ended = max(depth + 1 - 6, 0)
    for k in range(begun, depth):
        fourth(order[k])
    for k in range(ended, depth):
        fifth(order[k])

    parts = as_.shape[0]
    size = tokens // parts
    out[:, columns(me.y)] = moe[...].astype(BF16)
    nearby, passed = {}, {}
    for k in range(parts):
        here = out.at[pl.ds(k * size, size), columns(me.y)]
        for j, y in enumerate((me.up, me.down)):
            nearby[k, j] = send(here, here, as_.at[k, j], ar.at[k, j], me.in_y(y))
    thin = quarter // 2
    for k in range(parts):
        for j, (origin, target) in enumerate(((me.down, me.up), (me.up, me.down))):
            nearby[k, j].wait_recv()
            lanes = pl.ds(pl.multiple_of(origin * quarter + j * thin, thin), thin)
            piece = out.at[pl.ds(k * size, size), lanes]
            passed[k, j] = send(piece, piece, as_.at[k, 2 + j], ar.at[k, 2 + j], me.in_y(target))
    for k in range(parts):
        for j in range(2):
            passed[k, j].wait_recv()

    core = me.a % 2
    across_x = me.a // 2
    chips = plane // 2
    count = sp_size // 2
    block = gp.shape[2]
    gp[...] = (
        lax.dot_general(out[...], mixer[...], TN, preferred_element_type=F32)
        .astype(BF16)
        .reshape(gp.shape)
    )
    between = send(
        gp.at[:, 1 - core], cbuf, cs.at[0], cr.at[0],
        (me.z * plane + across_x * 2 + 1 - core, me.y),
    )
    loads[5].wait()
    d_mixer = jnp.dot(out[...], wo[...], preferred_element_type=F32)
    g_outer[...] = d_mixer * conv[...]
    dext[pl.ds(0, tokens), :] = d_mixer * outer[...].astype(F32)
    trail = send(dext.at[pl.ds(0, 8)], dext.at[pl.ds(tokens, 8)], hs.at[1], hr.at[1], before)

    between.wait_recv()
    summed = gp[:, core].astype(F32) + cbuf[...].astype(F32)
    hx[...] = summed.astype(BF16).reshape(hx.shape)
    over_x = []
    for d in range(1, chips):
        target = (across_x + d) % chips
        over_x.append(
            send(
                hx.at[:, target], xbuf.at[d - 1], gs.at[d - 1], gr.at[d - 1],
                (me.z * plane + target * 2 + core, me.y),
            )
        )

    trail.wait_recv()
    dext[pl.ds(tokens, 8), :] = jnp.where(me.sp == sp_size - 1, 0.0, dext[pl.ds(tokens, 8), :])
    d_mixed = (
        taps[2:3, :] * dext[pl.ds(0, tokens), :]
        + taps[1:2, :] * dext[pl.ds(1, tokens), :]
        + taps[0:1, :] * dext[pl.ds(2, tokens), :]
    )
    g_inner[...] = d_mixed * convin[...].astype(F32)
    g_convin[...] = d_mixed * inner[...].astype(F32)

    summed = hx[:, across_x].astype(F32)
    for d in range(1, chips):
        over_x[d - 1].wait_recv()
        summed += xbuf[d - 1].astype(F32)
    hz[...] = summed
    over_z = []
    for i, d in enumerate(me.dz):
        over_z.append(send(hz.at[(me.z + d) % depth], zsum.at[i], ts.at[i], tr.at[i], me.in_z(d)))
    total = hz[me.z]
    for i, copy in enumerate(over_z):
        copy.wait_recv()
        total += zsum[i]
    g_out[...] = total
    for copy in sent:
        copy.wait_send()


def shards(
    out_cotangent,
    stream,
    route_ids,
    route_weights,
    gate_proj,
    up_proj,
    down_proj,
    outer_gate,
    inner_gate,
    conv_input,
    conv_taps,
    out_proj,
):
    sp = lax.axis_size("sp")
    plane = plane_size(sp)
    depth = sp // plane
    tokens, width = stream.shape
    cap = 4 * tokens // sp
    chunk = plane * cap
    slots = depth * chunk
    quarter = width // NY
    hidden = gate_proj.shape[2]
    channels = outer_gate.shape[1]
    parts = 4
    block = width // sp
    vmem = pl.BlockSpec(memory_space=pltpu.VMEM)
    hbm = pl.BlockSpec(memory_space=pl.ANY)

    def dma(*shape):
        return pltpu.SemaphoreType.DMA(shape)

    def bf16(*shape):
        return pltpu.VMEM(shape, BF16)

    def f32(*shape):
        return pltpu.VMEM(shape, F32)

    def shape(dims, kind):
        return jax.ShapeDtypeStruct(dims, kind)

    grads = pl.pallas_call(
        functools.partial(layer_kernel, sp, cap),
        name="layer",
        out_shape=(
            shape((width, hidden), BF16),
            shape((width, hidden), BF16),
            shape((hidden, width), BF16),
            shape((block, channels), F32),
            shape((tokens, channels), F32),
            shape((tokens, channels), F32),
            shape((tokens, channels), F32),
        ),
        in_specs=[vmem] * 6 + [hbm] * 6,
        out_specs=(vmem,) * 7,
        scratch_shapes=[
            bf16(tokens, quarter),
            bf16(tokens, quarter),
            bf16(2 * tokens, quarter),
            bf16(width, 2 * hidden),
            bf16(hidden, width),
            bf16(width, channels),
            bf16(depth, plane, 2, cap, quarter),
            bf16(depth - 1, plane, 2, cap, quarter),
            bf16(2, slots, width),
            bf16(slots, hidden),
            bf16(slots, 2 * hidden),
            bf16(slots, width),
            bf16(depth, chunk, quarter),
            bf16(depth, chunk, quarter),
            bf16(depth, 2, chunk // 2, quarter),
            bf16(depth, 2, chunk // 2, quarter),
            bf16(depth, plane, cap, quarter),
            bf16(depth - 1, plane, cap, quarter),
            bf16(depth, plane, cap, quarter),
            f32(tokens, quarter),
            bf16(tokens, width),
            f32(tokens + 8, channels),
            f32(tokens + 8, channels),
            bf16(tokens, channels),
            f32(tokens, channels),
            bf16(sp // 2, 2, block, channels),
            bf16(sp // 2, block, channels),
            bf16(depth, plane // 2, block, channels),
            bf16(max(plane // 2 - 1, 1), depth, block, channels),
            f32(depth, block, channels),
            f32(depth - 1, block, channels),
            dma(6),
            dma(depth - 1),
            dma(depth - 1),
            dma(depth, plane - 1),
            dma(depth, plane - 1),
            dma(depth, 4),
            dma(depth, 4),
            dma(depth, 6),
            dma(depth, 6),
            dma(depth - 1),
            dma(depth - 1),
            dma(depth, plane - 1),
            dma(depth, plane - 1),
            dma(parts, 4),
            dma(parts, 4),
            dma(2),
            dma(2),
            dma(1),
            dma(1),
            dma(max(plane // 2 - 1, 1)),
            dma(max(plane // 2 - 1, 1)),
            dma(depth - 1),
            dma(depth - 1),
        ],
        compiler_params=pltpu.CompilerParams(
            collective_id=0, has_side_effects=True, vmem_limit_bytes=60 * 1024 * 1024
        ),
    )(
        route_ids, route_weights, outer_gate, inner_gate, conv_input, conv_taps,
        out_cotangent, stream, gate_proj[0], up_proj[0], down_proj[0], out_proj,
    )
    return (grads[0][None], grads[1][None], grads[2][None], *grads[3:])


def solution(mesh):
    placed = (
        P("sp", None),
        P("sp", None),
        P("sp", None),
        P("sp", None),
        P("sp", None, "tp"),
        P("sp", None, "tp"),
        P("sp", "tp", None),
        P("sp", "tp"),
        P("sp", "tp"),
        P("sp", "tp"),
        P(None, "tp"),
        P(None, "tp"),
    )
    return jax.shard_map(
        shards,
        mesh=mesh,
        in_specs=placed,
        out_specs=(
            P("sp", None, "tp"),
            P("sp", None, "tp"),
            P("sp", "tp", None),
            P("sp", "tp"),
            P("sp", "tp"),
            P("sp", "tp"),
            P("sp", "tp"),
        ),
        check_vma=False,
    )
```

time: 353 us -> 183 us (0.52)
  Pallas kernels: 0 us -> 171 us
  waiting for transfers between devices: 137 us -> 0 us
  blocking collectives: 85.6 us -> 0 us
  starting transfers between devices: 42.6 us -> 0 us
  local copies, waits for them, and re-layouts: 34.6 us -> 10.4 us
  matrix products: 22.2 us -> 0 us
  other arithmetic: 15.4 us -> 0 us
  between operations: 14.5 us -> 0.67 us
    pallas_call x0 -> x1, Pallas kernels: none -> 171 us  [shards(): pl.pallas_call(functools.partial(layer_kernel, sp, cap), name='layer', ou...]
    all_to_all x2 -> x0, blocking collectives: 85.6 us -> none  [the longest x1 51.4 us: summed_on_arrival(): lax.all_to_all(pieces, axis, split_axis=0, concat_axis=0, tiled=True)]
    all_gather x1 -> x0, waiting for transfers between devices: 82.7 us -> none  [sent_together(): out = lax.all_gather(both, axis, axis=dim, tiled=True)]
    all_to_all x4 -> x0, waiting for transfers between devices: 54.1 us -> none  [the longest x1 28.1 us: shards(): lax.all_to_all(share.reshape(sp_devices, capacity, quarter), 'sp', split_...]
    all_to_all x4 -> x0, starting transfers between devices: 36 us -> none  [the longest x1 13.2 us: shards(): lax.all_to_all(part_input, 'sp', split_axis=0, concat_axis=0, tiled=True)]
    dot_general x10 -> x0, matrix products: 22.2 us -> none  [the longest x1 5.14 us: shards(): lax.dot_general(hidden, rows_grad, over_rows, preferred_element_type=jnp....]
    gather x4 -> x0, local copies, waits for them, and re-layouts: 17.3 us -> none  [the longest x1 6.01 us: shards(): jnp.concatenate([stream, zero_row], axis=0)[slot_token]]
    unnamed x34 -> x25, local copies, waits for them, and re-layouts: 2.44 us -> 10.4 us
  transfers between devices with their start and end apart: 7 -> 0, of which waited for: 6 -> 0; matrix products, arithmetic and copies ran while one was open for 8% -> 0% of each run, Pallas kernels for 0% -> 0%
where the time goes in v2:
time: 183 us; the launch traced here: 182 us
  Pallas kernels  171 us (93%)
  local copies, waits for them, and re-layouts  10.4 us (6%)
    pallas_call x1, Pallas kernels, shards(): pl.pallas_call(functools.partial(layer_kernel, sp, cap), name='layer', ou...  171 us
    unnamed x25, local copies, waits for them, and re-layouts  10.4 us

profile of v2, /device:TPU:1, one launch (start us, length us, event | category | flops | bytes accessed | tf_op | source)
XLA Modules:
  0.0 182.4 jit_solution(5197522964263165079)
XLA Ops:
  0.6 0.0 copy-start.6
  0.6 0.7 copy-done.6
  1.3 0.0 copy-start.7
  1.3 0.8 copy.19.ids
  2.1 0.0 copy-done.7
  2.1 0.8 copy.20.weights
  2.9 171.3 %layer.1 = (bf16[2048,256]{1,0:T(8,128)(2,1)}, bf16[2048,256]{1,0:T(8,128)(2,1)}, bf16[256,2048]{1,0:T(8,128)(2,1)}, f32[32,128]{1,0:T(8,128)}, f32[256,128]{1,0...) custom-call(s32[256,2]{1,0:T(8,128)} %copy.19.ids, f32[256,2]{1,0:T(8,128)} %copy.20.weights, bf16[256,128]{1,0:T(8,128)(2,1)} %outer.1, ...), custom_call_target="tpu_custom_call" | custom-call | tf_op jit(solution)/shard_map/layer/pallas_call | solution.py:486
  174.3 0.0 copy-start.1
  174.3 2.4 %copy.28 = bf16[1,2048,256]{2,1,0:T(8,128)(2,1)} copy(bf16[1,2048,256]{2,1,0:T(8,128)(2,1)} %bitcast.8) | data formatting | bytes 2097152
  176.6 0.0 copy-done.1
  176.6 0.0 copy-start
  176.6 1.0 copy.29
  177.6 0.6 copy-done
  178.2 0.0 copy-start.5
  178.2 0.0 copy-start.4
  178.2 1.0 copy.30
  179.2 0.0 copy-done.5
  179.2 0.6 copy.31
  179.8 0.0 copy-done.4
  179.8 0.0 copy-start.3
  179.8 0.7 copy.32
  180.5 0.3 copy-done.3
  180.8 0.0 copy-start.2
  180.8 0.7 copy.33
  181.4 0.3 copy-done.2
  181.7 0.7 copy.34
Async XLA Ops:
  0.6 0.7 copy-start.6
  1.3 0.8 copy-start.7
  174.3 2.4 %copy-start.1 = (bf16[2048,256]{1,0:T(8,128)(2,1)S(1)}, bf16[2048,256]{1,0:T(8,128)(2,1)}, u32[]{:S(2)}) copy-start(bf16[2048,256]{1,0:T(8,128)(2,1)} %get-tuple-element.15) | copy-start | bytes 3145732
  176.6 1.6 copy-start
  178.2 1.0 copy-start.5
  178.2 1.6 copy-start.4
  179.8 1.0 copy-start.3
  180.8 1.0 copy-start.2

commit v3 on v2

--- a/solution.py
+++ b/solution.py
@@ -46,34 +46,21 @@
         self.dz = offsets(self.depth)
         self.da = list(range(1, self.plane))
 
-    def in_z(self, d):
-        return (((self.z + d) % self.depth) * self.plane + self.a, self.y)
-
-    def in_plane(self, d):
-        return (self.z * self.plane + (self.a + d) % self.plane, self.y)
+    def at(self, d, k):
+        plane = self.plane
+        return (((self.z + d) % self.depth) * plane + (self.a + k) % plane, self.y)
 
     def in_y(self, y):
         return (self.sp, y)
 
-    def meet(self, partners):
-        barrier = pltpu.get_barrier_semaphore()
-        for where in partners:
-            pl.semaphore_signal(barrier, inc=1, device_id=where, device_id_type=MESH)
-        pl.semaphore_wait(barrier, len(partners))
-
-    def all_partners(self):
-        return (
-            [self.in_z(d) for d in self.dz]
-            + [self.in_plane(d) for d in self.da]
-            + [self.in_y(self.up), self.in_y(self.down)]
-        )
-
 
 ORDERS = {
-    8: "B0 S0 B1 B2 B3 B4 Y0 B5 B6 B7 S1 S2 R0 Y1 Y2 R1 S3 S4 Y3 Y4 R2 F0 F1 D0 S5 S6 R3 Y5 Y6 R4 "
-    "F2 F3 D1 S7 Y7 R5 R6 F4 F5 D2 R7 F6 F7 D3",
-    2: "B0 S0 B1 Y0 S1 R0 Y1 R1 F0 F1 D0",
+    8: "S0 S1 S2 Y0 S3 S4 Y1 Y2 R0 R1 S5 S6 R2 Y3 Y4 R3 S7 R4 Y5 Y6 R5 X1 X2 X0 Y7 R6 R7 F4 F5 D2 P5 P4 "
+    "F2 F3 D1 F6 F7 D3 P7 P6 F0 F1 D0",
+    2: "S0 S1 Y0 Y1 R0 X0 R1 F0 F1 D0 P1 P0",
 }
+NEAR = {8: 3, 2: 1}
+RETURNS = {8: (5, 4, 7, 6, 3, 2, 1, 0), 2: (1, 0)}
 NT = (((1,), (1,)), ((), ()))
 TN = (((0,), (0,)), ((), ()))
 
@@ -84,15 +71,15 @@
     ids, weights, outer, inner, convin, taps,
     cotangent, stream, w_gate, w_up, w_down, w_out,
     g_gate, g_up, g_down, g_out, g_outer, g_inner, g_convin,
-    xq, ctq, scaled, wgu, wd, wo,
-    snd, zbuf, rows, hid, dgu, part,
-    gotup, gotdown, relays, sums, share, retz, ret, moe, out,
+    xall, ctq, scaled, wgu, wd, wo,
+    snd, wide_snd, rows, hid, dgu, part,
+    gotup, gotdown, relays, sums, share, ret, moe, out,
     ext, dext, mixer, conv, gp, cbuf, hx, xbuf, hz, zsum,
-    local, zs, zr, xs, xr, ys, yr, rs, rr, bs, br, ps, pr, as_, ar, hs, hr, cs, cr, gs, gr, ts, tr,
+    local, xs, xr, ws, wr, ys, yr, rs, rr, ps, pr, as_, ar, hs, hr, cs, cr, gs, gr, ts, tr,
 ):
     me = Place(sp_size)
     plane, depth = me.plane, me.depth
-    tokens, quarter = xq.shape
+    tokens, quarter = ctq.shape
     width = quarter * NY
     hidden = wd.shape[0]
     chunk = plane * cap
@@ -100,7 +87,10 @@
     slots = depth * chunk
     distances = [0] + me.dz
     after, before = ((me.sp + 1) % sp_size, me.y), ((me.sp + sp_size - 1) % sp_size, me.y)
+    others = [(i, k) for i in range(depth) for k in range(plane) if i + k > 0]
+    near = NEAR[depth]
     sent = []
+    groups = []
 
     def columns(y):
         return pl.ds(pl.multiple_of(y * quarter, quarter), quarter)
@@ -112,7 +102,7 @@
         return copy
 
     loads = [
-        pltpu.make_async_copy(stream.at[:, columns(me.y)], xq, local.at[0]),
+        pltpu.make_async_copy(stream, xall, local.at[0]),
         pltpu.make_async_copy(cotangent.at[:, columns(me.y)], ctq, local.at[1]),
         pltpu.make_async_copy(w_gate, wgu.at[:, pl.ds(0, hidden)], local.at[2]),
         pltpu.make_async_copy(w_up, wgu.at[:, pl.ds(hidden, hidden)], local.at[3]),
@@ -123,7 +113,7 @@
         copy.start()
 
     barrier = pltpu.get_barrier_semaphore()
-    partners = me.all_partners() + [after, before]
+    partners = [me.at(distances[i], k) for i, k in others] + [me.in_y(me.up), me.in_y(me.down)]
     for where in partners:
         pl.semaphore_signal(barrier, inc=1, device_id=where, device_id_type=MESH)
 
@@ -132,12 +122,16 @@
 
     square = (tokens, tokens)
     row, col = iota(square, 0), iota(square, 1)
-    ids_col = ids[...]
-    ids_row = lax.dot_general(
-        ids_col.astype(F32).astype(BF16), (row == col).astype(F32).astype(BF16), TN, preferred_element_type=F32
-    ).astype(jnp.int32)
+    ids_row = ids[...]
+    upright = [
+        jnp.broadcast_to(a[k : k + 1, :], (128, tokens)).T
+        for a in (ids_row.astype(F32), weights[...])
+        for k in range(2)
+    ]
+    ids_col = [a[:, :1].astype(jnp.int32) for a in upright[:2]]
+    weight_col = [a[:, :1] for a in upright[2:]]
     by_col = [
-        (iota((tokens, sp_size), 1) == ids_col[:, k : k + 1]).astype(F32) for k in range(2)
+        (iota((tokens, sp_size), 1) == ids_col[k]).astype(F32) for k in range(2)
     ]
     by_row = [
         (iota((sp_size, tokens), 0) == ids_row[k : k + 1, :]).astype(F32) for k in range(2)
@@ -153,7 +147,7 @@
     place_col, place_row = [], []
     for k in range(2):
         rank = jnp.sum(by_col[k] * count_col, axis=1, keepdims=True).astype(jnp.int32)
-        place_col.append(ids_col[:, k : k + 1] * cap + rank)
+        place_col.append(ids_col[k] * cap + rank)
         rank = jnp.sum(by_row[k] * count_row, axis=0, keepdims=True).astype(jnp.int32)
         place_row.append(ids_row[k : k + 1, :] * cap + rank)
 
@@ -164,71 +158,104 @@
     loads[1].wait()
     for k in range(2):
         scaled[pl.ds(k * tokens, tokens), :] = (
-            weights[:, k : k + 1] * ctq[...].astype(F32)
+            weight_col[k] * ctq[...].astype(F32)
         ).astype(BF16)
-
-    pl.semaphore_wait(barrier, len(partners))
 
     def base(i):
         return ((me.z + distances[i]) % depth) * chunk
-
-    along_z = {}
 
     def build(i):
         slot = base(i) + iota((chunk, tokens), 0)
         hits = [(slot == place_row[k]).astype(F32) for k in range(2)]
-        picked = jnp.dot(
-            (hits[0] + hits[1]).astype(BF16), xq[...], preferred_element_type=F32
-        ).astype(BF16)
-        snd[i, :, 0] = picked.reshape(plane, cap, quarter)
+        both = (hits[0] + hits[1]).astype(BF16)
+        if i < near:
+            picked = jnp.dot(both, xall[...], preferred_element_type=F32).astype(BF16)
+            wide_snd[i] = picked.reshape(plane, cap, width)
+        else:
+            picked = jnp.dot(both, xall[:, columns(me.y)], preferred_element_type=F32).astype(BF16)
+            snd[i, :, 0] = picked.reshape(plane, cap, quarter)
         picked = jnp.dot(
             jnp.concatenate(hits, axis=1).astype(BF16), scaled[...], preferred_element_type=F32
         ).astype(BF16)
         snd[i, :, 1] = picked.reshape(plane, cap, quarter)
-        if i > 0:
-            along_z[i] = send(
-                snd.at[i], zbuf.at[i - 1], zs.at[i - 1], zr.at[i - 1], me.in_z(distances[i])
-            )
-
-    in_plane = {}
-
-    def spread(i):
+
+    def group(i, sends, out_of, send_sem, recv_sem):
+        for k in range(plane):
+            if i + k > 0:
+                src, dst = sends(k)
+                remote(src, dst, send_sem, recv_sem, me.at(*out_of(k))).start()
+
+    def whole(ref, send_sem, recv_sem):
+        return remote(ref, ref, send_sem, recv_sem, me.in_y(me.up))
+
+    def block(i, k):
+        return pl.ds((i * plane + k) * cap, cap)
+
+    def blocks(i):
+        return pl.ds(cap, chunk - cap) if i == 0 else pl.ds(i * chunk, chunk)
+
+    def those(ref, i):
+        return ref.at[0, pl.ds(0, plane - 1)] if i == 0 else ref.at[i]
+
+    def outward(i):
+        return lambda k: (distances[i], k)
+
+    def ship(i):
+        if i < near:
+            def sends(k):
+                target = (me.a + k) % plane
+                return snd.at[i, target, 1], rows.at[1, block(i, k), columns(me.y)]
+        else:
+            def sends(k):
+                target = (me.a + k) % plane
+                return snd.at[i, target], rows.at[:, block(i, k), columns(me.y)]
+        group(i, sends, outward(i), xs.at[i], xr.at[i])
+        ref = snd.at[:, :, 1] if i < near else snd
+        groups.append(whole(those(ref, i), xs.at[i], xr.at[i]))
         if i == 0:
-            block = snd.at[0]
-        else:
-            along_z[i].wait_recv()
-            block = zbuf.at[i - 1]
-        for d in me.da:
-            in_plane[i, d] = send(
-                block.at[(me.a + d) % plane],
-                rows.at[:, pl.ds((i * plane + d) * cap, cap), columns(me.y)],
-                xs.at[i, d - 1],
-                xr.at[i, d - 1],
-                me.in_plane(d),
-            )
-        rows[:, pl.ds(i * chunk, cap), columns(me.y)] = block[me.a]
+            rows[1, pl.ds(0, cap), columns(me.y)] = snd[0, me.a, 1]
+            rows[0, pl.ds(0, cap), :] = wide_snd[0, me.a]
+
+    def ship_wide(i):
+        def sends(k):
+            return wide_snd.at[i, (me.a + k) % plane], rows.at[0, block(i, k), :]
+
+        group(i, sends, outward(i), ws.at[i], wr.at[i])
+        groups.append(whole(those(wide_snd, i), ws.at[i], wr.at[i]))
+
+    for i in range(depth):
+        build(i)
+    pl.semaphore_wait(barrier, len(partners))
 
     direct, relayed = {}, {}
 
     def round_y(i):
-        for d in me.da:
-            in_plane[i, d].wait_recv()
-        here = rows.at[:, pl.ds(i * chunk, chunk), columns(me.y)]
+        arrays = 1 if i < near else slice(None)
+        whole(rows.at[arrays, blocks(i), columns(me.y)], xs.at[i], xr.at[i]).wait_recv()
+        here = rows.at[arrays, pl.ds(i * chunk, chunk), columns(me.y)]
         for j, y in enumerate((me.up, me.down)):
             direct[i, j] = send(here, here, ys.at[i, j], yr.at[i, j], me.in_y(y))
 
     def relay(i):
         for j, (origin, target) in enumerate(((me.down, me.up), (me.up, me.down))):
             direct[i, j].wait_recv()
-            piece = rows.at[j, pl.ds(i * chunk, chunk), columns(origin)]
+            if i < near:
+                piece = rows.at[1, pl.ds(i * chunk + j * half, half), columns(origin)]
+            else:
+                piece = rows.at[j, pl.ds(i * chunk, chunk), columns(origin)]
             relayed[i, j] = send(piece, piece, ys.at[i, 2 + j], yr.at[i, 2 + j], me.in_y(target))
 
     def finish(i):
         for j in range(2):
             relayed[i, j].wait_recv()
+        if i < near:
+            whole(rows.at[0, blocks(i), :], ws.at[i], wr.at[i]).wait_recv()
+
+    ready = []
 
     def expert(g):
-        if g == 0:
+        if not ready:
+            ready.append(True)
             for k in range(2, 5):
                 loads[k].wait()
         here = pl.ds(g * 2 * chunk, 2 * chunk)
@@ -244,10 +271,6 @@
             dgu[here, :], wgu[...], NT, preferred_element_type=F32
         ).astype(BF16)
 
-    jobs = {"B": build, "S": spread, "Y": round_y, "R": relay, "F": finish, "D": expert}
-    for name in ORDERS[depth].split():
-        jobs[name[0]](int(name[1:]))
-
     got = {}
 
     def first(i):
@@ -260,6 +283,12 @@
             (3, part.at[low, columns(me.up)], gotdown.at[i, lo], me.up),
         ):
             got[i, j] = send(src, dst, rs.at[i, j], rr.at[i, j], me.in_y(y))
+
+    jobs = {
+        "S": ship, "X": ship_wide, "Y": round_y, "R": relay, "F": finish, "D": expert, "P": first,
+    }
+    for name in ORDERS[depth].split():
+        jobs[name[0]](int(name[1:]))
 
     def second(i):
         low, high = pl.ds(i * chunk, half), pl.ds(i * chunk + half, half)
@@ -274,8 +303,6 @@
             ).astype(BF16)
             got[i, 4 + j] = send(sums.at[i, j], dst, rs.at[i, 4 + j], rr.at[i, 4 + j], me.in_y(y))
 
-    back = {}
-
     def third(i):
         for j in range(2, 6):
             got[i, j].wait_recv()
@@ -285,30 +312,17 @@
             + gotdown[i].astype(F32)
         ).astype(BF16)
         share[i] = total.reshape(plane, cap, quarter)
-        if i > 0:
-            back[i] = send(
-                share.at[i], retz.at[i - 1], bs.at[i - 1], br.at[i - 1],
-                me.in_z(depth - distances[i]),
-            )
-
-    spreads = {}
+        if i == 0:
+            ret[0, me.a] = share[0, 0]
+
+        def sends(k):
+            return share.at[i, k], ret.at[i, me.a]
+
+        group(i, sends, lambda k: (depth - distances[i], plane - k), ps.at[i], pr.at[i])
+        groups.append(whole(those(share, i), ps.at[i], pr.at[i]))
 
     def fourth(i):
-        if i > 0:
-            back[i].wait_recv()
-            block = retz.at[i - 1]
-        else:
-            block = share.at[0]
-        for d in me.da:
-            spreads[i, d] = send(
-                block.at[d], ret.at[i, me.a], ps.at[i, d - 1], pr.at[i, d - 1],
-                me.in_plane(plane - d),
-            )
-        ret[i, me.a] = block[0]
-
-    def fifth(i):
-        for d in me.da:
-            spreads[i, d].wait_recv()
+        whole(those(ret, i), ps.at[i], pr.at[i]).wait_recv()
         slot = base(i) + iota((tokens, chunk), 1)
         hit = ((slot == place_col[0]) | (slot == place_col[1])).astype(F32).astype(BF16)
         moe[...] += jnp.dot(hit, ret[i].reshape(chunk, quarter), preferred_element_type=F32)
@@ -319,9 +333,9 @@
     def weight_grads(t):
         cols = pl.ds(t * wide, wide)
         both = lax.dot_general(rows[0, :, cols], dgu[...], TN, preferred_element_type=F32)
-        g_gate[cols, :] = both[:, :hidden].astype(BF16)
-        g_up[cols, :] = both[:, hidden:].astype(BF16)
-        g_down[:, cols] = lax.dot_general(
+        g_gate[0, cols, :] = both[:, :hidden].astype(BF16)
+        g_up[0, cols, :] = both[:, hidden:].astype(BF16)
+        g_down[0, :, cols] = lax.dot_general(
             hid[...], rows[1, :, cols], TN, preferred_element_type=F32
         ).astype(BF16)
 
@@ -336,13 +350,13 @@
         conv[...] = conv_out
         mixer[...] = (outer[...].astype(F32) * conv_out).astype(BF16)
 
-    order = list(range(depth - 1, -1, -1))
+    order = RETURNS[depth]
     moe[...] = ctq[...].astype(F32)
-    first(order[0])
-    first(order[1])
     halo = send(ext.at[pl.ds(tokens, 8)], ext.at[pl.ds(0, 8)], hs.at[0], hr.at[0], after)
+    lag = 5
+    early = min(4, depth)
     for step in range(depth + 1):
-        if step + 2 < depth:
+        if step + 2 < depth and step + 2 >= early:
             first(order[step + 2])
         if step < depth:
             second(order[step])
@@ -352,16 +366,10 @@
             weight_grads(step)
         if step == 1:
             convolution()
-        if step >= 5:
-            fourth(order[step - 5])
-        if step >= 6:
-            fifth(order[step - 6])
-    begun = max(depth + 1 - 5, 0)
-    ended = max(depth + 1 - 6, 0)
-    for k in range(begun, depth):
+        if step >= lag:
+            fourth(order[step - lag])
+    for k in range(max(depth + 1 - lag, 0), depth):
         fourth(order[k])
-    for k in range(ended, depth):
-        fifth(order[k])
 
     parts = as_.shape[0]
     size = tokens // parts
@@ -432,13 +440,13 @@
     hz[...] = summed
     over_z = []
     for i, d in enumerate(me.dz):
-        over_z.append(send(hz.at[(me.z + d) % depth], zsum.at[i], ts.at[i], tr.at[i], me.in_z(d)))
+        over_z.append(send(hz.at[(me.z + d) % depth], zsum.at[i], ts.at[i], tr.at[i], me.at(d, 0)))
     total = hz[me.z]
     for i, copy in enumerate(over_z):
         copy.wait_recv()
         total += zsum[i]
     g_out[...] = total
-    for copy in sent:
+    for copy in sent + groups:
         copy.wait_send()
 
 
@@ -467,6 +475,7 @@
     hidden = gate_proj.shape[2]
     channels = outer_gate.shape[1]
     parts = 4
+    near = NEAR[depth]
     block = width // sp
     vmem = pl.BlockSpec(memory_space=pltpu.VMEM)
     hbm = pl.BlockSpec(memory_space=pl.ANY)
@@ -480,32 +489,30 @@
     def f32(*shape):
         return pltpu.VMEM(shape, F32)
 
-    def shape(dims, kind):
-        return jax.ShapeDtypeStruct(dims, kind)
-
-    grads = pl.pallas_call(
+    shapes = (
+        ((1, width, hidden), BF16),
+        ((1, width, hidden), BF16),
+        ((1, hidden, width), BF16),
+        ((block, channels), F32),
+        ((tokens, channels), F32),
+        ((tokens, channels), F32),
+        ((tokens, channels), F32),
+    )
+    return pl.pallas_call(
         functools.partial(layer_kernel, sp, cap),
         name="layer",
-        out_shape=(
-            shape((width, hidden), BF16),
-            shape((width, hidden), BF16),
-            shape((hidden, width), BF16),
-            shape((block, channels), F32),
-            shape((tokens, channels), F32),
-            shape((tokens, channels), F32),
-            shape((tokens, channels), F32),
-        ),
+        out_shape=tuple(pltpu.VMEM(*s) for s in shapes),
         in_specs=[vmem] * 6 + [hbm] * 6,
         out_specs=(vmem,) * 7,
         scratch_shapes=[
-            bf16(tokens, quarter),
+            bf16(tokens, width),
             bf16(tokens, quarter),
             bf16(2 * tokens, quarter),
             bf16(width, 2 * hidden),
             bf16(hidden, width),
             bf16(width, channels),
             bf16(depth, plane, 2, cap, quarter),
-            bf16(depth - 1, plane, 2, cap, quarter),
+            bf16(near, plane, cap, width),
             bf16(2, slots, width),
             bf16(slots, hidden),
             bf16(slots, 2 * hidden),
@@ -515,7 +522,6 @@
             bf16(depth, 2, chunk // 2, quarter),
             bf16(depth, 2, chunk // 2, quarter),
             bf16(depth, plane, cap, quarter),
-            bf16(depth - 1, plane, cap, quarter),
             bf16(depth, plane, cap, quarter),
             f32(tokens, quarter),
             bf16(tokens, width),
@@ -530,18 +536,16 @@
             f32(depth, block, channels),
             f32(depth - 1, block, channels),
             dma(6),
-            dma(depth - 1),
-            dma(depth - 1),
-            dma(depth, plane - 1),
-            dma(depth, plane - 1),
+            dma(depth),
+            dma(depth),
+            dma(near),
+            dma(near),
             dma(depth, 4),
             dma(depth, 4),
             dma(depth, 6),
             dma(depth, 6),
-            dma(depth - 1),
-            dma(depth - 1),
-            dma(depth, plane - 1),
-            dma(depth, plane - 1),
+            dma(depth),
+            dma(depth),
             dma(parts, 4),
             dma(parts, 4),
             dma(2),
@@ -557,10 +561,9 @@
             collective_id=0, has_side_effects=True, vmem_limit_bytes=60 * 1024 * 1024
         ),
     )(
-        route_ids, route_weights, outer_gate, inner_gate, conv_input, conv_taps,
+        route_ids.T, route_weights.T, outer_gate, inner_gate, conv_input, conv_taps,
         out_cotangent, stream, gate_proj[0], up_proj[0], down_proj[0], out_proj,
     )
-    return (grads[0][None], grads[1][None], grads[2][None], *grads[3:])
 
 
 def solution(mesh):

time: 183 us -> 168 us (0.918)
  Pallas kernels: 171 us -> 161 us
  local copies, waits for them, and re-layouts: 10.4 us -> 5.48 us
    pallas_call x1, Pallas kernels: 171 us -> 161 us  [shards(): pl.pallas_call(functools.partial(layer_kernel, sp, cap), name='layer', ou...]
    unnamed x25 -> x7, local copies, waits for them, and re-layouts: 10.4 us -> 5.48 us
where the time goes in v3:
time: 168 us
  Pallas kernels  161 us (96%)
  local copies, waits for them, and re-layouts  5.48 us (3%)
    pallas_call x1, Pallas kernels, shards(): pl.pallas_call(functools.partial(layer_kernel, sp, cap), name='layer', ou...  161 us
    unnamed x7, local copies, waits for them, and re-layouts  5.48 us

profile of v3, /device:TPU:1, one launch (start us, length us, event | category | flops | bytes accessed | tf_op | source)
XLA Modules:
  0.0 167.5 jit_solution(3197192622339601755)
XLA Ops:
  0.6 161.4 %layer.1 = (bf16[1,2048,256]{2,1,0:T(8,128)(2,1)S(1)}, bf16[1,2048,256]{2,1,0:T(8,128)(2,1)S(1)}, bf16[1,256,2048]{2,1,0:T(8,128)(2,1)S(1)}, f32[32,128]{1,0:T(8...) custom-call(s32[2,256]{1,0:T(2,128)} %bitcast.8, f32[2,256]{1,0:T(2,128)} %bitcast.9, ...), custom_call_target="tpu_custom_call" | custom-call | tf_op jit(solution)/shard_map/layer/pallas_call | solution.py:501
  162.1 1.0 copy.26
  163.0 0.6 copy.29
  163.6 0.7 copy.30
  164.3 0.7 copy.31
  164.9 0.7 copy.32
  165.6 1.0 copy.27
  166.6 1.0 copy.28

commit v4 on v3

--- a/solution.py
+++ b/solution.py
@@ -14,7 +14,7 @@
 
 
 def plane_size(sp):
-    return 8 if sp % 8 == 0 and sp > 8 else 2
+    return sp // 8
 
 
 def offsets(n):
@@ -55,12 +55,11 @@
 
 
 ORDERS = {
-    8: "S0 S1 S2 Y0 S3 S4 Y1 Y2 R0 R1 S5 S6 R2 Y3 Y4 R3 S7 R4 Y5 Y6 R5 X1 X2 X0 Y7 R6 R7 F4 F5 D2 P5 P4 "
-    "F2 F3 D1 F6 F7 D3 P7 P6 F0 F1 D0",
-    2: "S0 S1 Y0 Y1 R0 X0 R1 F0 F1 D0 P1 P0",
+    8: "S0 S1 S2 W0 Y0 S3 S4 S5 S6 Y1 Y2 R0 C0 R1 S7 X0 R2 Y3 Y4 R3 R4 Y5 Y6 R5 Y7 R6 R7 F4 F5 D2 P5 P4 "
+    "F2 F3 D1 F6 F7 D3 F0 F1 D0",
 }
-NEAR = {8: 3, 2: 1}
-RETURNS = {8: (5, 4, 7, 6, 3, 2, 1, 0), 2: (1, 0)}
+NEAR = {8: 1}
+RETURNS = {8: (5, 4, 7, 6, 3, 2, 1, 0)}
 NT = (((1,), (1,)), ((), ()))
 TN = (((0,), (0,)), ((), ()))
 
@@ -73,7 +72,7 @@
     g_gate, g_up, g_down, g_out, g_outer, g_inner, g_convin,
     xall, ctq, scaled, wgu, wd, wo,
     snd, wide_snd, rows, hid, dgu, part,
-    gotup, gotdown, relays, sums, share, ret, moe, out,
+    gotup, gotdown, relays, sums, share, ret, moe, wall, mall, dsend, dgot,
     ext, dext, mixer, conv, gp, cbuf, hx, xbuf, hz, zsum,
     local, xs, xr, ws, wr, ys, yr, rs, rr, ps, pr, as_, ar, hs, hr, cs, cr, gs, gr, ts, tr,
 ):
@@ -113,9 +112,20 @@
         copy.start()
 
     barrier = pltpu.get_barrier_semaphore()
-    partners = [me.at(distances[i], k) for i, k in others] + [me.in_y(me.up), me.in_y(me.down)]
+    partners = [me.at(distances[i], k) for i, k in others] + [me.in_y(y) for y in (me.up, me.across, me.down)]
     for where in partners:
         pl.semaphore_signal(barrier, inc=1, device_id=where, device_id_type=MESH)
+
+    layers = depth // NY
+    holder = me.z // layers == me.y
+    for k in range(depth):
+        where = (k * plane + me.a, me.z // layers)
+
+        @pl.when(jnp.logical_not(jnp.logical_and(holder, me.z == k)))
+        def _():
+            pl.semaphore_signal(barrier, inc=1, device_id=where, device_id_type=MESH)
+
+    greetings = len(partners) + depth - holder.astype(jnp.int32)
 
     def iota(shape, dim):
         return lax.broadcasted_iota(jnp.int32, shape, dim)
@@ -225,7 +235,8 @@
 
     for i in range(depth):
         build(i)
-    pl.semaphore_wait(barrier, len(partners))
+    loads[5].wait()
+    pl.semaphore_wait(barrier, greetings)
 
     direct, relayed = {}, {}
 
@@ -284,8 +295,44 @@
         ):
             got[i, j] = send(src, dst, rs.at[i, j], rr.at[i, j], me.in_y(y))
 
+    channels = mixer.shape[1]
+
+    def lanes(y):
+        return pl.ds(pl.multiple_of(y * channels, channels), channels)
+
+    def to_others(kind, src_of, dst):
+        for o in range(1, NY):
+            y = (me.y + o) % NY
+            exchanged[kind, o] = send(
+                src_of(y), dst(o), as_.at[kind, o - 1], ar.at[kind, o - 1], me.in_y(y)
+            )
+
+    exchanged = {}
+
+    def share_weights(_):
+        exchanged["halo"] = send(
+            ext.at[pl.ds(tokens, 8)], ext.at[pl.ds(0, 8)], hs.at[0], hr.at[0], after
+        )
+        to_others(0, lambda y: wo.at[columns(y), :], lambda o: wall.at[:, lanes(me.y)])
+        wall[:, lanes(me.y)] = wo[columns(me.y), :]
+
+    def convolution(_):
+        exchanged["halo"].wait_recv()
+        ext[pl.ds(0, 8), :] = jnp.where(me.sp == 0, 0.0, ext[pl.ds(0, 8), :])
+        conv_out = (
+            taps[0:1, :] * ext[pl.ds(6, tokens), :]
+            + taps[1:2, :] * ext[pl.ds(7, tokens), :]
+            + taps[2:3, :] * ext[pl.ds(8, tokens), :]
+        )
+        conv[...] = conv_out
+        mixer_out = (outer[...].astype(F32) * conv_out).astype(BF16)
+        mixer[...] = mixer_out
+        mall[:, lanes(me.y)] = mixer_out
+        to_others(1, lambda y: mixer, lambda o: mall.at[:, lanes(me.y)])
+
     jobs = {
         "S": ship, "X": ship_wide, "Y": round_y, "R": relay, "F": finish, "D": expert, "P": first,
+        "W": share_weights, "C": convolution,
     }
     for name in ORDERS[depth].split():
         jobs[name[0]](int(name[1:]))
@@ -339,22 +386,9 @@
             hid[...], rows[1, :, cols], TN, preferred_element_type=F32
         ).astype(BF16)
 
-    def convolution():
-        halo.wait_recv()
-        ext[pl.ds(0, 8), :] = jnp.where(me.sp == 0, 0.0, ext[pl.ds(0, 8), :])
-        conv_out = (
-            taps[0:1, :] * ext[pl.ds(6, tokens), :]
-            + taps[1:2, :] * ext[pl.ds(7, tokens), :]
-            + taps[2:3, :] * ext[pl.ds(8, tokens), :]
-        )
-        conv[...] = conv_out
-        mixer[...] = (outer[...].astype(F32) * conv_out).astype(BF16)
-
     order = RETURNS[depth]
     moe[...] = ctq[...].astype(F32)
-    halo = send(ext.at[pl.ds(tokens, 8)], ext.at[pl.ds(0, 8)], hs.at[0], hr.at[0], after)
-    lag = 5
-    early = min(4, depth)
+    early = 2
     for step in range(depth + 1):
         if step + 2 < depth and step + 2 >= early:
             first(order[step + 2])
@@ -364,55 +398,36 @@
             third(order[step - 1])
         if step < tiles:
             weight_grads(step)
-        if step == 1:
-            convolution()
-        if step >= lag:
-            fourth(order[step - lag])
-    for k in range(max(depth + 1 - lag, 0), depth):
+    for k in range(depth):
         fourth(order[k])
 
-    parts = as_.shape[0]
-    size = tokens // parts
-    out[:, columns(me.y)] = moe[...].astype(BF16)
-    nearby, passed = {}, {}
-    for k in range(parts):
-        here = out.at[pl.ds(k * size, size), columns(me.y)]
-        for j, y in enumerate((me.up, me.down)):
-            nearby[k, j] = send(here, here, as_.at[k, j], ar.at[k, j], me.in_y(y))
-    thin = quarter // 2
-    for k in range(parts):
-        for j, (origin, target) in enumerate(((me.down, me.up), (me.up, me.down))):
-            nearby[k, j].wait_recv()
-            lanes = pl.ds(pl.multiple_of(origin * quarter + j * thin, thin), thin)
-            piece = out.at[pl.ds(k * size, size), lanes]
-            passed[k, j] = send(piece, piece, as_.at[k, 2 + j], ar.at[k, 2 + j], me.in_y(target))
-    for k in range(parts):
-        for j in range(2):
-            passed[k, j].wait_recv()
-
+    for o in range(1, NY):
+        exchanged[1, o].wait_recv()
+        exchanged[0, o].wait_recv()
+    stream_grad = moe[...].astype(BF16)
     core = me.a % 2
     across_x = me.a // 2
     chips = plane // 2
-    count = sp_size // 2
-    block = gp.shape[2]
     gp[...] = (
-        lax.dot_general(out[...], mixer[...], TN, preferred_element_type=F32)
+        lax.dot_general(stream_grad, mall[...], TN, preferred_element_type=F32)
         .astype(BF16)
         .reshape(gp.shape)
     )
     between = send(
-        gp.at[:, 1 - core], cbuf, cs.at[0], cr.at[0],
+        gp.at[:, :, 1 - core], cbuf, cs.at[0], cr.at[0],
         (me.z * plane + across_x * 2 + 1 - core, me.y),
     )
-    loads[5].wait()
-    d_mixer = jnp.dot(out[...], wo[...], preferred_element_type=F32)
-    g_outer[...] = d_mixer * conv[...]
-    dext[pl.ds(0, tokens), :] = d_mixer * outer[...].astype(F32)
-    trail = send(dext.at[pl.ds(0, 8)], dext.at[pl.ds(tokens, 8)], hs.at[1], hr.at[1], before)
+    for o in range(1, NY):
+        y = (me.y + o) % NY
+        dsend[o - 1] = jnp.dot(
+            stream_grad, wall[:, lanes(y)], preferred_element_type=F32
+        ).astype(BF16)
+    to_others(2, lambda y: dsend.at[(y - me.y + NY) % NY - 1], lambda o: dgot.at[o - 1])
+    d_mixer = jnp.dot(stream_grad, wall[:, lanes(me.y)], preferred_element_type=F32)
 
     between.wait_recv()
-    summed = gp[:, core].astype(F32) + cbuf[...].astype(F32)
-    hx[...] = summed.astype(BF16).reshape(hx.shape)
+    summed = gp[:, :, core].astype(F32) + cbuf[...].astype(F32)
+    hx[...] = summed.astype(BF16)
     over_x = []
     for d in range(1, chips):
         target = (across_x + d) % chips
@@ -423,6 +438,36 @@
             )
         )
 
+    for o in range(1, NY):
+        exchanged[2, o].wait_recv()
+        d_mixer += dgot[o - 1].astype(F32)
+    dext[pl.ds(0, tokens), :] = d_mixer * outer[...].astype(F32)
+    trail = send(dext.at[pl.ds(0, 8)], dext.at[pl.ds(tokens, 8)], hs.at[1], hr.at[1], before)
+    g_outer[...] = d_mixer * conv[...]
+
+    summed = hx[:, across_x].astype(F32)
+    for d in range(1, chips):
+        over_x[d - 1].wait_recv()
+        summed += xbuf[d - 1].astype(F32)
+    to_owner = []
+    for k in range(layers):
+        for y in range(NY):
+            hz[k, y] = summed[k, :, y * channels : (y + 1) * channels].astype(BF16)
+            owner = layers * me.y + k
+            mine = jnp.logical_and(owner == me.z, me.y == y)
+            copy = remote(
+                hz.at[k, y], zsum.at[me.z], ts.at[k, y], tr.at[me.z], (owner * plane + me.a, y)
+            )
+            to_owner.append((mine, copy))
+
+            @pl.when(mine)
+            def _():
+                zsum[me.z] = hz[k, y]
+
+            @pl.when(jnp.logical_not(mine))
+            def _():
+                copy.start()
+
     trail.wait_recv()
     dext[pl.ds(tokens, 8), :] = jnp.where(me.sp == sp_size - 1, 0.0, dext[pl.ds(tokens, 8), :])
     d_mixed = (
@@ -433,21 +478,21 @@
     g_inner[...] = d_mixed * convin[...].astype(F32)
     g_convin[...] = d_mixed * inner[...].astype(F32)
 
-    summed = hx[:, across_x].astype(F32)
-    for d in range(1, chips):
-        over_x[d - 1].wait_recv()
-        summed += xbuf[d - 1].astype(F32)
-    hz[...] = summed
-    over_z = []
-    for i, d in enumerate(me.dz):
-        over_z.append(send(hz.at[(me.z + d) % depth], zsum.at[i], ts.at[i], tr.at[i], me.at(d, 0)))
-    total = hz[me.z]
-    for i, copy in enumerate(over_z):
-        copy.wait_recv()
-        total += zsum[i]
+    for k in range(depth):
+        @pl.when(jnp.logical_not(jnp.logical_and(holder, me.z == k)))
+        def _():
+            remote(zsum.at[k], zsum.at[k], ts.at[0, 0], tr.at[k], me.in_y(me.up)).wait_recv()
+
+    total = zsum[0].astype(F32)
+    for k in range(1, depth):
+        total += zsum[k].astype(F32)
     g_out[...] = total
     for copy in sent + groups:
         copy.wait_send()
+    for mine, copy in to_owner:
+        @pl.when(jnp.logical_not(mine))
+        def _():
+            copy.wait_send()
 
 
 def shards(
@@ -474,7 +519,8 @@
     quarter = width // NY
     hidden = gate_proj.shape[2]
     channels = outer_gate.shape[1]
-    parts = 4
+    layers = depth // NY
+    chips = plane // 2
     near = NEAR[depth]
     block = width // sp
     vmem = pl.BlockSpec(memory_space=pltpu.VMEM)
@@ -524,17 +570,20 @@
             bf16(depth, plane, cap, quarter),
             bf16(depth, plane, cap, quarter),
             f32(tokens, quarter),
-            bf16(tokens, width),
+            bf16(quarter, NY * channels),
+            bf16(tokens, NY * channels),
+            bf16(NY - 1, tokens, channels),
+            bf16(NY - 1, tokens, channels),
             f32(tokens + 8, channels),
             f32(tokens + 8, channels),
             bf16(tokens, channels),
             f32(tokens, channels),
-            bf16(sp // 2, 2, block, channels),
-            bf16(sp // 2, block, channels),
-            bf16(depth, plane // 2, block, channels),
-            bf16(max(plane // 2 - 1, 1), depth, block, channels),
-            f32(depth, block, channels),
-            f32(depth - 1, block, channels),
+            bf16(layers, chips, 2, block, NY * channels),
+            bf16(layers, chips, block, NY * channels),
+            bf16(layers, chips, block, NY * channels),
+            bf16(max(chips - 1, 1), layers, block, NY * channels),
+            bf16(layers, NY, block, channels),
+            bf16(depth, block, channels),
             dma(6),
             dma(depth),
             dma(depth),
@@ -546,16 +595,16 @@
             dma(depth, 6),
             dma(depth),
             dma(depth),
-            dma(parts, 4),
-            dma(parts, 4),
+            dma(3, NY - 1),
+            dma(3, NY - 1),
             dma(2),
             dma(2),
             dma(1),
             dma(1),
-            dma(max(plane // 2 - 1, 1)),
-            dma(max(plane // 2 - 1, 1)),
-            dma(depth - 1),
-            dma(depth - 1),
+            dma(max(chips - 1, 1)),
+            dma(max(chips - 1, 1)),
+            dma(layers, NY),
+            dma(depth),
         ],
         compiler_params=pltpu.CompilerParams(
             collective_id=0, has_side_effects=True, vmem_limit_bytes=60 * 1024 * 1024

time: 168 us -> 154 us (0.917)
  Pallas kernels: 161 us -> 147 us
    pallas_call x1, Pallas kernels: 161 us -> 147 us  [shards(): pl.pallas_call(functools.partial(layer_kernel, sp, cap), name='layer', ou...]
where the time goes in v4:
time: 154 us; the launch traced here: 153 us
  Pallas kernels  147 us (95%)
  local copies, waits for them, and re-layouts  5.48 us (4%)
    pallas_call x1, Pallas kernels, shards(): pl.pallas_call(functools.partial(layer_kernel, sp, cap), name='layer', ou...  147 us
    unnamed x7, local copies, waits for them, and re-layouts  5.48 us

profile of v4, /device:TPU:1, one launch (start us, length us, event | category | flops | bytes accessed | tf_op | source)
XLA Modules:
  0.0 153.4 jit_solution(4497624276341967577)
XLA Ops:
  0.6 147.3 %layer.1 = (bf16[1,2048,256]{2,1,0:T(8,128)(2,1)S(1)}, bf16[1,2048,256]{2,1,0:T(8,128)(2,1)S(1)}, bf16[1,256,2048]{2,1,0:T(8,128)(2,1)S(1)}, f32[32,128]{1,0:T(8...) custom-call(s32[2,256]{1,0:T(2,128)} %bitcast.8, f32[2,256]{1,0:T(2,128)} %bitcast.9, ...), custom_call_target="tpu_custom_call" | custom-call | tf_op jit(solution)/shard_map/layer/pallas_call | solution.py:547
  147.9 1.0 copy.26
  148.9 0.6 copy.29
  149.5 0.7 copy.30
  150.2 0.7 copy.31
  150.8 0.7 copy.32
  151.5 1.0 copy.27
  152.4 1.0 copy.28

commit v5 on v4

--- a/solution.py
+++ b/solution.py
@@ -55,10 +55,10 @@
 
 
 ORDERS = {
-    8: "S0 S1 S2 W0 Y0 S3 S4 S5 S6 Y1 Y2 R0 C0 R1 S7 X0 R2 Y3 Y4 R3 R4 Y5 Y6 R5 Y7 R6 R7 F4 F5 D2 P5 P4 "
-    "F2 F3 D1 F6 F7 D3 F0 F1 D0",
+    8: "S1 S2 W0 S3 S4 S5 S6 Y1 Y2 S7 C0 R1 X0 R2 X1 X2 Y3 Y4 R3 R4 Y5 Y6 R5 Y7 R6 R7 F4 F5 D2 P5 P4 "
+    "F6 F7 D3 F2 F3 D1 F0 F1 D0",
 }
-NEAR = {8: 1}
+NEAR = {8: 3}
 RETURNS = {8: (5, 4, 7, 6, 3, 2, 1, 0)}
 NT = (((1,), (1,)), ((), ()))
 TN = (((0,), (0,)), ((), ()))
@@ -70,16 +70,16 @@
     ids, weights, outer, inner, convin, taps,
     cotangent, stream, w_gate, w_up, w_down, w_out,
     g_gate, g_up, g_down, g_out, g_outer, g_inner, g_convin,
-    xall, ctq, scaled, wgu, wd, wo,
-    snd, wide_snd, rows, hid, dgu, part,
+    xall, call, scaled, wgu, wd, wo,
+    snd, full_snd, wide_snd, rows, hid, dgu, part,
     gotup, gotdown, relays, sums, share, ret, moe, wall, mall, dsend, dgot,
     ext, dext, mixer, conv, gp, cbuf, hx, xbuf, hz, zsum,
     local, xs, xr, ws, wr, ys, yr, rs, rr, ps, pr, as_, ar, hs, hr, cs, cr, gs, gr, ts, tr,
 ):
     me = Place(sp_size)
     plane, depth = me.plane, me.depth
-    tokens, quarter = ctq.shape
-    width = quarter * NY
+    tokens, width = call.shape
+    quarter = width // NY
     hidden = wd.shape[0]
     chunk = plane * cap
     half = chunk // 2
@@ -102,7 +102,7 @@
 
     loads = [
         pltpu.make_async_copy(stream, xall, local.at[0]),
-        pltpu.make_async_copy(cotangent.at[:, columns(me.y)], ctq, local.at[1]),
+        pltpu.make_async_copy(cotangent, call, local.at[1]),
         pltpu.make_async_copy(w_gate, wgu.at[:, pl.ds(0, hidden)], local.at[2]),
         pltpu.make_async_copy(w_up, wgu.at[:, pl.ds(hidden, hidden)], local.at[3]),
         pltpu.make_async_copy(w_down, wd, local.at[4]),
@@ -168,7 +168,7 @@
     loads[1].wait()
     for k in range(2):
         scaled[pl.ds(k * tokens, tokens), :] = (
-            weight_col[k] * ctq[...].astype(F32)
+            weight_col[k] * call[...].astype(F32)
         ).astype(BF16)
 
     def base(i):
@@ -178,15 +178,21 @@
         slot = base(i) + iota((chunk, tokens), 0)
         hits = [(slot == place_row[k]).astype(F32) for k in range(2)]
         both = (hits[0] + hits[1]).astype(BF16)
+        apart = jnp.concatenate(hits, axis=1).astype(BF16)
+        here = columns(me.y)
+        if i == 0:
+            picked = jnp.dot(both, xall[...], preferred_element_type=F32).astype(BF16)
+            full_snd[:, 0] = picked.reshape(plane, cap, width)
+            picked = jnp.dot(apart, scaled[...], preferred_element_type=F32).astype(BF16)
+            full_snd[:, 1] = picked.reshape(plane, cap, width)
+            return
         if i < near:
             picked = jnp.dot(both, xall[...], preferred_element_type=F32).astype(BF16)
-            wide_snd[i] = picked.reshape(plane, cap, width)
+            wide_snd[i - 1] = picked.reshape(plane, cap, width)
         else:
-            picked = jnp.dot(both, xall[:, columns(me.y)], preferred_element_type=F32).astype(BF16)
+            picked = jnp.dot(both, xall[:, here], preferred_element_type=F32).astype(BF16)
             snd[i, :, 0] = picked.reshape(plane, cap, quarter)
-        picked = jnp.dot(
-            jnp.concatenate(hits, axis=1).astype(BF16), scaled[...], preferred_element_type=F32
-        ).astype(BF16)
+        picked = jnp.dot(apart, scaled[:, here], preferred_element_type=F32).astype(BF16)
         snd[i, :, 1] = picked.reshape(plane, cap, quarter)
 
     def group(i, sends, out_of, send_sem, recv_sem):
@@ -222,16 +228,19 @@
         group(i, sends, outward(i), xs.at[i], xr.at[i])
         ref = snd.at[:, :, 1] if i < near else snd
         groups.append(whole(those(ref, i), xs.at[i], xr.at[i]))
-        if i == 0:
-            rows[1, pl.ds(0, cap), columns(me.y)] = snd[0, me.a, 1]
-            rows[0, pl.ds(0, cap), :] = wide_snd[0, me.a]
 
     def ship_wide(i):
         def sends(k):
-            return wide_snd.at[i, (me.a + k) % plane], rows.at[0, block(i, k), :]
+            target = (me.a + k) % plane
+            if i == 0:
+                return full_snd.at[target], rows.at[:, block(i, k), :]
+            return wide_snd.at[i - 1, target], rows.at[0, block(i, k), :]
 
         group(i, sends, outward(i), ws.at[i], wr.at[i])
-        groups.append(whole(those(wide_snd, i), ws.at[i], wr.at[i]))
+        sent_refs = full_snd.at[pl.ds(0, plane - 1)] if i == 0 else wide_snd.at[i - 1]
+        groups.append(whole(sent_refs, ws.at[i], wr.at[i]))
+        if i == 0:
+            rows[:, pl.ds(0, cap), :] = full_snd[me.a]
 
     for i in range(depth):
         build(i)
@@ -257,10 +266,12 @@
             relayed[i, j] = send(piece, piece, ys.at[i, 2 + j], yr.at[i, 2 + j], me.in_y(target))
 
     def finish(i):
-        for j in range(2):
-            relayed[i, j].wait_recv()
+        if i > 0:
+            for j in range(2):
+                relayed[i, j].wait_recv()
         if i < near:
-            whole(rows.at[0, blocks(i), :], ws.at[i], wr.at[i]).wait_recv()
+            arrays = slice(None) if i == 0 else 0
+            whole(rows.at[arrays, blocks(i), :], ws.at[i], wr.at[i]).wait_recv()
 
     ready = []
 
@@ -387,7 +398,7 @@
         ).astype(BF16)
 
     order = RETURNS[depth]
-    moe[...] = ctq[...].astype(F32)
+    moe[...] = call[:, columns(me.y)].astype(F32)
     early = 2
     for step in range(depth + 1):
         if step + 2 < depth and step + 2 >= early:
@@ -552,13 +563,14 @@
         out_specs=(vmem,) * 7,
         scratch_shapes=[
             bf16(tokens, width),
-            bf16(tokens, quarter),
-            bf16(2 * tokens, quarter),
+            bf16(tokens, width),
+            bf16(2 * tokens, width),
             bf16(width, 2 * hidden),
             bf16(hidden, width),
             bf16(width, channels),
             bf16(depth, plane, 2, cap, quarter),
-            bf16(near, plane, cap, width),
+            bf16(plane, 2, cap, width),
+            bf16(max(near - 1, 1), plane, cap, width),
             bf16(2, slots, width),
             bf16(slots, hidden),
             bf16(slots, 2 * hidden),

time: 154 us -> 146 us (0.948)
  Pallas kernels: 147 us -> 140 us
    pallas_call x1, Pallas kernels: 147 us -> 140 us  [shards(): pl.pallas_call(functools.partial(layer_kernel, sp, cap), name='layer', ou...]
where the time goes in v5:
time: 146 us
  Pallas kernels  140 us (96%)
  local copies, waits for them, and re-layouts  5.48 us (4%)
    pallas_call x1, Pallas kernels, shards(): pl.pallas_call(functools.partial(layer_kernel, sp, cap), name='layer', ou...  140 us
    unnamed x7, local copies, waits for them, and re-layouts  5.48 us

profile of v5, /device:TPU:1, one launch (start us, length us, event | category | flops | bytes accessed | tf_op | source)
XLA Modules:
  0.0 146.3 jit_solution(7491561972049222572)
XLA Ops:
  0.6 140.2 %layer.1 = (bf16[1,2048,256]{2,1,0:T(8,128)(2,1)S(1)}, bf16[1,2048,256]{2,1,0:T(8,128)(2,1)S(1)}, bf16[1,256,2048]{2,1,0:T(8,128)(2,1)S(1)}, f32[32,128]{1,0:T(8...) custom-call(s32[2,256]{1,0:T(2,128)} %bitcast.8, f32[2,256]{1,0:T(2,128)} %bitcast.9, ...), custom_call_target="tpu_custom_call" | custom-call | tf_op jit(solution)/shard_map/layer/pallas_call | solution.py:558
  140.9 1.0 copy.26
  141.8 0.6 copy.29
  142.4 0.7 copy.30
  143.1 0.7 copy.31
  143.7 0.7 copy.32
  144.4 1.0 copy.27
  145.4 1.0 copy.28

commit v6 on v5

--- a/solution.py
+++ b/solution.py
@@ -55,11 +55,11 @@
 
 
 ORDERS = {
-    8: "S1 S2 W0 S3 S4 S5 S6 Y1 Y2 S7 C0 R1 X0 R2 X1 X2 Y3 Y4 R3 R4 Y5 Y6 R5 Y7 R6 R7 F4 F5 D2 P5 P4 "
-    "F6 F7 D3 F2 F3 D1 F0 F1 D0",
+    8: "S1 S2 W0 S3 S4 S5 S6 Y1 Y2 S7 C0 R1 X0 R2 X1 X2 Y3 Y4 R3 R4 Y5 Y6 R5 Y7 R6 F4 F5 D2 R7 P5 P4 "
+    "F2 F3 D1 F6 F7 D3 F0 F1 D0",
 }
 NEAR = {8: 3}
-RETURNS = {8: (5, 4, 7, 6, 3, 2, 1, 0)}
+RETURNS = {8: (5, 4, 6, 7, 3, 2, 1, 0)}
 NT = (((1,), (1,)), ((), ()))
 TN = (((0,), (0,)), ((), ()))
 

time: 146 us -> 144 us (0.986)
  Pallas kernels: 140 us -> 138 us
    pallas_call x1, Pallas kernels: 140 us -> 138 us  [shards(): pl.pallas_call(functools.partial(layer_kernel, sp, cap), name='layer', ou...]
where the time goes in v6:
time: 144 us
  Pallas kernels  138 us (96%)
  local copies, waits for them, and re-layouts  5.48 us (4%)
    pallas_call x1, Pallas kernels, shards(): pl.pallas_call(functools.partial(layer_kernel, sp, cap), name='layer', ou...  138 us
    unnamed x7, local copies, waits for them, and re-layouts  5.48 us

profile of v6, /device:TPU:1, one launch (start us, length us, event | category | flops | bytes accessed | tf_op | source)
XLA Modules:
  0.0 144.2 jit_solution(2903880562478699440)
XLA Ops:
  0.6 138.1 %layer.1 = (bf16[1,2048,256]{2,1,0:T(8,128)(2,1)S(1)}, bf16[1,2048,256]{2,1,0:T(8,128)(2,1)S(1)}, bf16[1,256,2048]{2,1,0:T(8,128)(2,1)S(1)}, f32[32,128]{1,0:T(8...) custom-call(s32[2,256]{1,0:T(2,128)} %bitcast.8, f32[2,256]{1,0:T(2,128)} %bitcast.9, ...), custom_call_target="tpu_custom_call" | custom-call | tf_op jit(solution)/shard_map/layer/pallas_call | solution.py:558
  138.7 1.0 copy.26
  139.7 0.6 copy.29
  140.3 0.7 copy.30
  141.0 0.7 copy.31
  141.6 0.7 copy.32
  142.3 1.0 copy.27
  143.2 1.0 copy.28
